TPU v7x, 128 devices: a whole 4x4x4 slice. The times are simulated.
128 devices in a mesh: sp: 16 (over z, x), dp: 8 (over y, core).
Axes of the slice: x: 4, y: 4, z: 4, core: 2. Of those that a mesh axis runs over, the one named last changes fastest.
Arguments:
- queries: bfloat16 [8, 2048, 2048], P('dp', 'sp'), may hold values from -9 to 9
- keys: bfloat16 [8, 2048, 512], P('dp', 'sp'), may hold values from -9 to 9
- values: bfloat16 [8, 2048, 512], P('dp', 'sp'), may hold values from -6 to 6
- out_grad: bfloat16 [8, 2048, 2048], P('dp', 'sp'), may hold values from -24 to 24
- layer_in: bfloat16 [8, 2048, 4096], P('dp', 'sp'), may hold values from -0.09375 to 0.09375
- key_weight: bfloat16 [4096, 512], P('dp'), may hold values from -0.09375 to 0.09375
- value_weight: bfloat16 [4096, 512], P('dp'), may hold values from -0.09375 to 0.09375
- query_gain: float32 [128], replicated, may hold values from 0.64 to 6.04
- key_gain: float32 [128], replicated, may hold values from 0.64 to 6.04
Outputs:
- grad_query: bfloat16 [8, 2048, 2048], P('dp', 'sp')
- grad_in: bfloat16 [8, 2048, 4096], P('dp', 'sp')
- grad_key_weight: float32 [4096, 512], P('dp')
- grad_value_weight: float32 [4096, 512], P('dp')
All inputs are finite; a program needn't handle non-finite values.
Results may differ from a plain program's by a relative error of at most 0.018.
The roundings to bfloat16 on the way count: a program that leaves them out, or rounds other values in their place, can miss the bound.
Values may be sent and summed in bfloat16 or wider, within the bound.
A program may use at most 128 MiB of HBM per device.

v0:
```python
from functools import partial
import math

import jax
import jax.numpy as jnp
from jax import lax
from jax.sharding import PartitionSpec as P

HEADS = 16
KV_HEADS = 4
HEAD_DIM = 128
GRID_W = 64


epsilon = 1e-06
rope_base = 10000.0


def sent_together(arrays, axis, dim, along):
    widths = [a.shape[along] for a in arrays]
    both = jnp.concatenate(arrays, axis=along)
    result = lax.all_gather(both, axis, axis=dim, tiled=True)
    return tuple(jnp.split(result, [sum(widths[:k]) for k in range(1, len(widths))], axis=along))


def padded_to(lines, peers):
    spare = -len(lines) % peers
    return jnp.pad(lines, [(0, spare)] + [(0, 0)] * (lines.ndim - 1))


def copy_for_each(array, axis):
    peers = lax.axis_size(axis)
    return lax.all_to_all(
        jnp.broadcast_to(array[None], (peers, *array.shape)), axis, 0, 0, tiled=True
    )


def laid_out(parts, dim):
    dims = list(parts.shape[1:])
    dims[dim] *= parts.shape[0]
    return jnp.moveaxis(parts, 0, dim).reshape(dims)


def collect(array, axis, dim):
    parts = copy_for_each(array, axis)
    return laid_out(parts, dim)


def cut_along(array, dim, peers):
    before, after = (array.shape[:dim], array.shape[dim + 1 :])
    return jnp.moveaxis(array.reshape(*before, peers, -1, *after), dim, 0)


def sum_at_owner(array, axis, dim):
    peers = lax.axis_size(axis)
    parts = lax.all_to_all(cut_along(array, dim, peers), axis, 0, 0, tiled=True)
    return jnp.sum(parts.astype(jnp.float32), axis=0)


def nested_sum(array, axes):
    lines = array.reshape(-1, array.shape[-1])
    padded = padded_to(lines, lax.axis_size(axes))
    whole = collect(sum_at_owner(padded, axes, 0).astype(jnp.bfloat16), axes, 0)
    return lax.slice_in_dim(whole, 0, len(lines)).reshape(array.shape).astype(jnp.float32)


def norm_rotate(vector, gain_vec, row_index, col_index):
    scaled = (
        vector * lax.rsqrt(jnp.mean(vector * vector, axis=-1, keepdims=True) + epsilon) * gain_vec
    )
    quarter = vector.shape[-1] // 4
    inverse = rope_base ** (-jnp.arange(quarter, dtype=jnp.float32) / quarter)
    pieces = []
    for offset, position in ((0, row_index), (2 * quarter, col_index)):
        angles = position.astype(jnp.float32)[:, None] * inverse[None, :]
        cosine = jnp.cos(angles)
        sine_part = jnp.sin(angles)
        first_half = scaled[:, offset : offset + quarter]
        second_half = scaled[:, offset + quarter : offset + 2 * quarter]
        pieces.append(first_half * cosine - second_half * sine_part)
        pieces.append(first_half * sine_part + second_half * cosine)
    return jnp.concatenate(pieces, axis=1)


def contract_cols(left_side, right_side):
    return lax.dot_general(
        left_side, right_side, (((1,), (1,)), ((), ())), preferred_element_type=jnp.float32
    )


def contract_rows(left_side, right_side):
    return lax.dot_general(
        left_side, right_side, (((0,), (0,)), ((), ())), preferred_element_type=jnp.float32
    )


def head_grads(query_rows, grad_rows, key_rows, value_rows, query_gain, key_gain):
    length = query_rows.shape[0]
    block_rows = math.gcd(length, 512)
    positions = jnp.arange(length, dtype=jnp.int32)
    row_index = positions // GRID_W
    col_index = positions % GRID_W
    q_rot, q_back = jax.vjp(
        partial(norm_rotate, gain_vec=query_gain, row_index=row_index, col_index=col_index),
        query_rows.astype(jnp.float32),
    )
    k_rot, k_back = jax.vjp(
        partial(norm_rotate, gain_vec=key_gain, row_index=row_index, col_index=col_index),
        key_rows.astype(jnp.float32),
    )
    q_bf = q_rot.astype(jnp.bfloat16)
    k_bf = k_rot.astype(jnp.bfloat16)
    score_scale = q_rot.shape[-1] ** (-0.5)

    def one_block(accums, block_index):
        k_acc, v_acc = accums
        row_start = block_index * block_rows
        q_block = lax.dynamic_slice_in_dim(q_bf, row_start, block_rows, 0)
        g_block = lax.dynamic_slice_in_dim(grad_rows, row_start, block_rows, 0)
        scores = contract_cols(q_block, k_bf) * score_scale
        shifted = jnp.exp(scores - jnp.max(scores, axis=1, keepdims=True))
        attn_probs = shifted / jnp.sum(shifted, axis=1, keepdims=True)
        probs_b = attn_probs.astype(jnp.bfloat16)
        attn_out = jnp.dot(probs_b, value_rows, preferred_element_type=jnp.float32)
        row_delta = jnp.sum(g_block.astype(jnp.float32) * attn_out, axis=1, keepdims=True)
        grad_probs = contract_cols(g_block, value_rows)
        grad_scores = (attn_probs * (grad_probs - row_delta)).astype(jnp.bfloat16)
        q_grad = jnp.dot(grad_scores, k_bf, preferred_element_type=jnp.float32) * score_scale
        k_acc = k_acc + contract_rows(grad_scores, q_block) * score_scale
        v_acc = v_acc + contract_rows(probs_b, g_block)
        return ((k_acc, v_acc), q_grad)

    zeros_init = jnp.zeros(query_rows.shape, jnp.float32)
    (k_acc, v_acc), q_grads = lax.scan(
        one_block, (zeros_init, zeros_init), jnp.arange(length // block_rows, dtype=jnp.int32)
    )
    grad_rq = q_grads.reshape(length, query_rows.shape[1])
    grad_q = q_back(grad_rq)[0].astype(jnp.bfloat16)
    grad_k = k_back(k_acc)[0].astype(jnp.bfloat16)
    return (grad_q, grad_k, v_acc.astype(jnp.bfloat16))


def on_device(
    queries, keys, values, out_grad, layer_in, key_weight, value_weight, query_gain, key_gain
):
    seq_count, tokens_here, _ = queries.shape
    model_width = layer_in.shape[2]
    group_size = HEADS // KV_HEADS
    kv_width = KV_HEADS * HEAD_DIM
    key_full, value_full = sent_together((key_weight, value_weight), "dp", 0, 1)
    query_part = queries.reshape(seq_count, tokens_here, HEADS, HEAD_DIM)
    grad_part = out_grad.reshape(seq_count, tokens_here, HEADS, HEAD_DIM)
    shape_wide = (seq_count, tokens_here, KV_HEADS, group_size, HEAD_DIM)
    key_part = jnp.broadcast_to(
        keys.reshape(seq_count, tokens_here, KV_HEADS, 1, HEAD_DIM), shape_wide
    ).reshape(seq_count, tokens_here, HEADS, HEAD_DIM)
    value_part = jnp.broadcast_to(
        values.reshape(seq_count, tokens_here, KV_HEADS, 1, HEAD_DIM), shape_wide
    ).reshape(seq_count, tokens_here, HEADS, HEAD_DIM)
    bundle = jnp.concatenate([query_part, grad_part, key_part, value_part], axis=3)
    arrived = lax.all_to_all(bundle, "sp", split_axis=2, concat_axis=1, tiled=True)
    arrived_seqs, length, head_count, _ = arrived.shape
    flat_heads = arrived.transpose(0, 2, 1, 3).reshape(
        arrived_seqs * head_count, length, 4 * HEAD_DIM
    )

    def one_item(one_head):
        grad_q, grad_k, grad_v = head_grads(
            one_head[:, :HEAD_DIM],
            one_head[:, HEAD_DIM : 2 * HEAD_DIM],
            one_head[:, 2 * HEAD_DIM : 3 * HEAD_DIM],
            one_head[:, 3 * HEAD_DIM :],
            query_gain,
            key_gain,
        )
        return jnp.concatenate([grad_q, grad_k, grad_v], axis=1)

    all_grads = lax.map(one_item, flat_heads)
    head_out = all_grads.reshape(arrived_seqs, head_count, length, 3 * HEAD_DIM).transpose(
        0, 2, 1, 3
    )
    token_grads = lax.all_to_all(head_out, "sp", split_axis=1, concat_axis=2, tiled=True)
    grad_query = token_grads[:, :, :, :HEAD_DIM].reshape(seq_count, tokens_here, HEADS * HEAD_DIM)

    def grouped(array):
        summed = jnp.sum(
            array.reshape(seq_count * tokens_here, KV_HEADS, group_size, HEAD_DIM).astype(
                jnp.float32
            ),
            axis=2,
        )
        return summed.astype(jnp.bfloat16).reshape(seq_count * tokens_here, kv_width)

    kv_grad = jnp.concatenate(
        [
            grouped(token_grads[:, :, :, HEAD_DIM : 2 * HEAD_DIM]),
            grouped(token_grads[:, :, :, 2 * HEAD_DIM :]),
        ],
        axis=1,
    )
    both_weights = jnp.concatenate([key_full, value_full], axis=1)
    grad_flat = contract_cols(kv_grad, both_weights)
    grad_in = grad_flat.astype(jnp.bfloat16).reshape(seq_count, tokens_here, model_width)
    flat_in = layer_in.reshape(seq_count * tokens_here, model_width)
    partial_sum = lax.psum_scatter(
        contract_rows(flat_in, kv_grad).astype(jnp.bfloat16), "dp", scatter_dimension=0, tiled=True
    )
    weight_grad = nested_sum(partial_sum, "sp")
    return (grad_query, grad_in, weight_grad[:, :kv_width], weight_grad[:, kv_width:])


def solution(mesh):
    in_specs = (
        P("dp", "sp", None),
        P("dp", "sp", None),
        P("dp", "sp", None),
        P("dp", "sp", None),
        P("dp", "sp", None),
        P("dp", None),
        P("dp", None),
        P(),
        P(),
    )
    out_specs = (P("dp", "sp", None), P("dp", "sp", None), P("dp", None), P("dp", None))
    return jax.shard_map(
        on_device, mesh=mesh, in_specs=in_specs, out_specs=out_specs, check_vma=False
    )
```

profile of v0, /device:TPU:1, one launch (start us, length us, event | category | flops | bytes accessed | tf_op | source)
XLA Modules:
  0.0 371.3 jit_solution(12669012684862657344)
XLA Ops:
  9.3 2.0 copy.71
  11.4 2.0 copy.72
  15.0 2.6 copy.75
  17.6 8.4 %all-to-all-start = ((bf16[1,128,16,512]{3,1,0,2:T(8,128)(2,1)}), bf16[1,128,16,512]{3,1,0,2:T(8,128)(2,1)S(1)}, u32[]{:S(2)}, u32[]{:S(2)}) async-start(bf16[1,128,16,512]{3,1,0,2:T(8,128)(2,1)} %copy.75), calls=%async_computation | async-start | bytes 4194304 | tf_op jit(solution)/shard_map/all_to_all | solution.py:161
  26.1 30.8 %all-to-all-done = bf16[1,128,16,512]{3,1,0,2:T(8,128)(2,1)S(1)} async-done(((bf16[1,128,16,512]{3,1,0,2:T(8,128)(2,1)}), bf16[1,128,16,512]{3,1,0,2:T(8,128)(2,1)S(1)}, u32[]{:S(2)}, u32[]{:S(2)}) %all-to-all-start) | async-done | bytes 2097184 | tf_op jit(solution)/shard_map/all_to_all | solution.py:161
  58.3 2.5 fusion.93
  63.1 2.6 fusion.56
  67.9 77.8 %while.24 = (s32[]{:T(128)}, f32[2048,128]{1,0:T(8,128)}, f32[2048,128]{1,0:T(8,128)}, f32[4,512,128]{2,1,0:T(8,128)}, s32[4]{0:T(128)S(1)}, /*index=5*/bf16[204...) while((s32[]{:T(128)}, f32[2048,128]{1,0:T(8,128)}, ...), condition=%wide.region_6.7_spmd.clone, body=%wide.region_2.6_spmd.clone.sunk | while | flops 1625815552 | bytes 93731832 | solution.py:134
  70.9 2.7 fusion.133
  73.8 3.2 fusion.134
  77.2 1.8 multiply_convert_fusion.2
  79.0 2.8 fusion.135
  81.8 2.5 fusion.136
  84.3 1.8 convolution_add_fusion.2
  89.0 2.7 fusion.133
  91.9 3.2 fusion.134
  95.3 1.8 multiply_convert_fusion.2
  97.1 3.2 fusion.135
  100.3 2.5 fusion.136
  102.8 3.1 convolution_add_fusion.2
  108.9 2.7 fusion.133
  111.8 3.2 fusion.134
  115.2 1.8 multiply_convert_fusion.2
  117.0 3.2 fusion.135
  120.2 2.5 fusion.136
  122.7 3.1 convolution_add_fusion.2
  128.8 2.7 fusion.133
  131.7 3.2 fusion.134
  135.1 1.8 multiply_convert_fusion.2
  136.9 3.2 fusion.135
  140.1 2.5 fusion.136
  142.5 3.1 convolution_add_fusion.2
  145.7 4.9 %fusion.95 = (f32[2048,32]{1,0:T(8,128)}, f32[2048,32]{1,0:T(8,128)}, f32[2048,32]{1,0:T(8,128)}, f32[2048,32]{1,0:T(8,128)S(1)}) fusion(f32[2048,128]{1,0:T(8,128)} %bitcast.71), kind=kLoop, calls=%fused_computation.137 | loop fusion | bytes 2097152 | tf_op jit(solution)/shard_map/while/body/eval_jaxpr/transpose(jvp())/split | solution.py:82
  152.2 2.3 copy.106
  154.5 2.2 copy.107
  159.0 4.0 %fusion.63 = (f32[2048,32]{0,1:T(8,128)S(1)}, f32[2048,32]{0,1:T(8,128)S(1)}, f32[2048,32]{0,1:T(8,128)S(1)}, f32[2048,32]{0,1:T(8,128)S(1)}, f32[2048,32]{0,1:T...) fusion(f32[2048,32]{0,1:T(8,128)} %copy.107, f32[2048,32]{0,1:T(8,128)} %copy.108, ...), kind=kLoop, calls=%fused_computation.95 | loop fusion | flops 1966080 | bytes 4210816 | tf_op jit(solution)/shard_map/while/body/eval_jaxpr/transpose(jvp())/add_any | solution.py:80
  164.9 2.2 copy.85
  168.4 5.7 %copy.87 = bf16[1,2048,1,384]{3,2,0,1:T(2,128)(2,1)} copy(bf16[1,2048,1,384]{1,3,2,0:T(8,128)(2,1)S(1)} %maximum_bitcast_fusion) | data formatting | bytes 3145728 | tf_op jit(solution)/shard_map/transpose;reshape | solution.py:179
  174.6 34.5 %reduce.3 = bf16[2048,384]{1,0:T(8,128)(2,1)S(1)} reduce(bf16[2048,1,1,384]{3,2,1,0:T(2,128)(2,1)} %bitcast.72, bf16[]{:T(256)} %broadcast.219), dimensions={1,2}, to_apply=%bitcast.40.reduce_sub_computation | reduce | bytes 3145730
  210.5 25.3 %all_to_all.43 = bf16[16,2,24576]{2,1,0:T(2,128)(2,1)S(1)} all-to-all(bf16[16,2,24576]{2,1,0:T(2,128)(2,1)} %reshape.148), channel_id=1, replica_groups=mesh['sp'=16,'dp'=8] {'sp'}, dimensions={0} | all-to-all | bytes 3145728 | tf_op jit(solution)/shard_map/all_to_all | solution.py:182
  235.8 6.3 %reshape.149 = bf16[2048,1,1,384]{3,2,1,0:T(2,128)(2,1)} reshape(bf16[16,2,24576]{2,1,0:T(2,128)(2,1)S(1)} %all_to_all.43) | data formatting | bytes 3145728
  242.1 2.1 copy.100
  245.9 5.5 %convert_bitcast_fusion = bf16[4096,1024]{0,1:T(8,128)(2,1)} fusion(bf16[1,128,4096]{2,1,0:T(8,128)(2,1)S(1)} %copy-done, bf16[128,512]{0,1:T(8,128)(2,1)S(1)} %bitcast.86, bf16[128,512]{0,1:T(8,128)(2,1)S(1)} %bitcast.84), kind=kOutput, calls=%fused_computation.21 | convolution fusion | flops 1078460416 | bytes 9699328 | tf_op jit(solution)/shard_map/dot_general | solution.py:92
  253.8 49.0 %reduce-scatter.2.cloned.1.call-done = bf16[512,1024]{0,1:T(8,128)(2,1)} async-done(((bf16[4096,1024]{0,1:T(8,128)(2,1)}), bf16[512,1024]{0,1:T(8,128)(2,1)}) %reduce-scatter.2.cloned.1.call-update) | async-done | bytes 1048592 | tf_op jit(solution)/shard_map/reduce_scatter | solution.py:205
  304.3 22.3 %all_to_all.44 = bf16[16,32,1024]{2,1,0:T(8,128)(2,1)S(1)} all-to-all(bf16[16,32,1024]{2,1,0:T(8,128)(2,1)S(1)} %bitcast.76), channel_id=1, replica_groups=mesh['sp'=16,'dp'=8] {'sp'}, dimensions={0} | all-to-all | bytes 2097152 | tf_op jit(solution)/shard_map/all_to_all | solution.py:56
  327.9 3.9 %all-to-all-start.3 = ((bf16[16,32,1024]{2,1,0:T(8,128)(2,1)}), bf16[16,32,1024]{2,1,0:T(8,128)(2,1)S(1)}, u32[]{:S(2)}, u32[]{:S(2)}) async-start(bf16[16,32,1024]{2,1,0:T(8,128)(2,1)} %broadcast_in_dim.70), calls=%async_computation.4 | async-start | bytes 2097152 | tf_op jit(solution)/shard_map/all_to_all | solution.py:33
  333.1 22.3 %all-gather.2.cloned.1.call-done = bf16[4096,1024]{1,0:T(8,128)(2,1)} async-done(((bf16[512,1024]{1,0:T(8,128)(2,1)}), bf16[4096,1024]{1,0:T(8,128)(2,1)}) %all-gather.2.cloned.1.call-update) | async-done | bytes 8388624 | tf_op jit(solution)/shard_map/all_gather | solution.py:22
  355.4 7.2 %fusion.13 = bf16[1,128,4096]{2,1,0:T(8,128)(2,1)} fusion(bf16[4096,1024]{1,0:T(8,128)(2,1)} %all-gather.2.cloned.1.call-done, bf16[128,512]{0,1:T(8,128)(2,1)S(1)} %bitcast.87, bf16[128,512]{0,1:T(8,128)(2,1)S(1)} %bitcast.85), kind=kOutput, calls=%fused_computation.23 | convolution fusion | flops 1074790400 | bytes 9699328 | tf_op jit(solution)/shard_map/dot_general | solution.py:86
  (176 shorter events, 39.3 us)
Async XLA Ops:
  7.2 238.7 %copy-start = (bf16[1,128,4096]{2,1,0:T(8,128)(2,1)S(1)}, bf16[1,128,4096]{2,1,0:T(8,128)(2,1)}, u32[]{:S(2)}) copy-start(bf16[1,128,4096]{2,1,0:T(8,128)(2,1)} %param.15) | copy-start | bytes 3145732
  17.6 39.4 %all-to-all-start = ((bf16[1,128,16,512]{3,1,0,2:T(8,128)(2,1)}), bf16[1,128,16,512]{3,1,0,2:T(8,128)(2,1)S(1)}, u32[]{:S(2)}, u32[]{:S(2)}) async-start(bf16[1,128,16,512]{3,1,0,2:T(8,128)(2,1)} %copy.75), calls=%async_computation | async-start | bytes 4194304 | tf_op jit(solution)/shard_map/all_to_all | solution.py:161
  26.0 276.8 %reduce-scatter.2.cloned.1.call-start = ((), (), s32[]{:S(2)}) async-start(), calls=%async_computation.6 | async-start | bytes 9437184 | tf_op jit(solution)/shard_map/reduce_scatter | solution.py:205
  58.3 4.4 %copy-start.21 = (f32[128]{0:T(128)S(1)}, f32[128]{0:T(128)}, u32[]{:S(2)}) copy-start(f32[128]{0:T(128)} %param.19) | copy-start | bytes 1540
  61.1 4.6 %copy-start.8 = (bf16[2048,128]{0,1:T(8,128)(2,1)}, bf16[2048,128]{0,1:T(8,128)(2,1)S(1)}, u32[]{:S(2)}) copy-start(bf16[2048,128]{0,1:T(8,128)(2,1)S(1)} %copy.102) | copy-start | bytes 1572868
  62.5 3.2 copy-start.10
  67.9 3.0 copy-start.5
  67.9 3.0 copy-start.13
  67.9 5.7 %copy-start.15 = (bf16[2048,128]{1,0:T(8,128)(2,1)}, bf16[2048,128]{1,0:T(8,128)(2,1)S(1)}, u32[]{:S(2)}) copy-start(bf16[2048,128]{1,0:T(8,128)(2,1)S(1)} %get-tuple-element.348) | copy-start | bytes 1572868 | tf_op jit(solution)/shard_map/while/body/eval_jaxpr/while
  67.9 5.8 %copy-start.3 = (bf16[2048,128]{1,0:T(8,128)(2,1)}, bf16[2048,128]{1,0:T(8,128)(2,1)S(1)}, u32[]{:S(2)}) copy-start(bf16[2048,128]{1,0:T(8,128)(2,1)S(1)} %get-tuple-element.349) | copy-start | bytes 1572868 | tf_op jit(solution)/shard_map/while/body/eval_jaxpr/while
  73.8 3.5 copy-start.1
  79.0 5.2 %copy-start.2 = (f32[512,2048]{1,0:T(8,128)S(1)}, f32[512,2048]{1,0:T(8,128)}, u32[]{:S(2)}) copy-start(f32[512,2048]{1,0:T(8,128)} %fusion.133) | copy-start | bytes 12582916 | tf_op jit(solution)/shard_map/while/body/eval_jaxpr/while
  86.0 3.0 copy-start.5
  86.0 3.0 copy-start.13
  86.1 5.7 %copy-start.15 = (bf16[2048,128]{1,0:T(8,128)(2,1)}, bf16[2048,128]{1,0:T(8,128)(2,1)S(1)}, u32[]{:S(2)}) copy-start(bf16[2048,128]{1,0:T(8,128)(2,1)S(1)} %get-tuple-element.348) | copy-start | bytes 1572868 | tf_op jit(solution)/shard_map/while/body/eval_jaxpr/while
  86.1 5.8 %copy-start.3 = (bf16[2048,128]{1,0:T(8,128)(2,1)}, bf16[2048,128]{1,0:T(8,128)(2,1)S(1)}, u32[]{:S(2)}) copy-start(bf16[2048,128]{1,0:T(8,128)(2,1)S(1)} %get-tuple-element.349) | copy-start | bytes 1572868 | tf_op jit(solution)/shard_map/while/body/eval_jaxpr/while
  91.9 3.5 copy-start.1
  97.1 5.6 %copy-start.2 = (f32[512,2048]{1,0:T(8,128)S(1)}, f32[512,2048]{1,0:T(8,128)}, u32[]{:S(2)}) copy-start(f32[512,2048]{1,0:T(8,128)} %fusion.133) | copy-start | bytes 12582916 | tf_op jit(solution)/shard_map/while/body/eval_jaxpr/while
  102.8 3.1 copy-start.4
  102.8 3.1 copy-start.6
  102.8 3.1 copy-start.14
  102.8 3.1 copy-start.16
  105.9 3.0 copy-start.5
  105.9 3.0 copy-start.13
  105.9 5.7 %copy-start.15 = (bf16[2048,128]{1,0:T(8,128)(2,1)}, bf16[2048,128]{1,0:T(8,128)(2,1)S(1)}, u32[]{:S(2)}) copy-start(bf16[2048,128]{1,0:T(8,128)(2,1)S(1)} %get-tuple-element.348) | copy-start | bytes 1572868 | tf_op jit(solution)/shard_map/while/body/eval_jaxpr/while
  105.9 5.8 %copy-start.3 = (bf16[2048,128]{1,0:T(8,128)(2,1)}, bf16[2048,128]{1,0:T(8,128)(2,1)S(1)}, u32[]{:S(2)}) copy-start(bf16[2048,128]{1,0:T(8,128)(2,1)S(1)} %get-tuple-element.349) | copy-start | bytes 1572868 | tf_op jit(solution)/shard_map/while/body/eval_jaxpr/while
  111.8 3.5 copy-start.1
  117.0 5.6 %copy-start.2 = (f32[512,2048]{1,0:T(8,128)S(1)}, f32[512,2048]{1,0:T(8,128)}, u32[]{:S(2)}) copy-start(f32[512,2048]{1,0:T(8,128)} %fusion.133) | copy-start | bytes 12582916 | tf_op jit(solution)/shard_map/while/body/eval_jaxpr/while
  122.6 3.1 copy-start.4
  122.6 3.1 copy-start.6
  122.6 3.1 copy-start.14
  122.6 3.1 copy-start.16
  125.8 3.0 copy-start.5
  125.8 3.0 copy-start.13
  125.8 5.7 %copy-start.15 = (bf16[2048,128]{1,0:T(8,128)(2,1)}, bf16[2048,128]{1,0:T(8,128)(2,1)S(1)}, u32[]{:S(2)}) copy-start(bf16[2048,128]{1,0:T(8,128)(2,1)S(1)} %get-tuple-element.348) | copy-start | bytes 1572868 | tf_op jit(solution)/shard_map/while/body/eval_jaxpr/while
  125.8 5.8 %copy-start.3 = (bf16[2048,128]{1,0:T(8,128)(2,1)}, bf16[2048,128]{1,0:T(8,128)(2,1)S(1)}, u32[]{:S(2)}) copy-start(bf16[2048,128]{1,0:T(8,128)(2,1)S(1)} %get-tuple-element.349) | copy-start | bytes 1572868 | tf_op jit(solution)/shard_map/while/body/eval_jaxpr/while
  131.7 3.5 copy-start.1
  136.9 5.6 %copy-start.2 = (f32[512,2048]{1,0:T(8,128)S(1)}, f32[512,2048]{1,0:T(8,128)}, u32[]{:S(2)}) copy-start(f32[512,2048]{1,0:T(8,128)} %fusion.133) | copy-start | bytes 12582916 | tf_op jit(solution)/shard_map/while/body/eval_jaxpr/while
  142.5 3.1 copy-start.4
  142.5 3.1 copy-start.6
  142.5 3.1 copy-start.14
  142.5 3.1 copy-start.16
  150.6 7.1 %copy-start.7 = (f32[2048,128]{1,0:T(8,128)S(1)}, f32[2048,128]{1,0:T(8,128)}, u32[]{:S(2)}) copy-start(f32[2048,128]{1,0:T(8,128)} %get-tuple-element.69) | copy-start | bytes 3145732
  157.7 5.3 %copy-start.11 = (bf16[2048,128]{0,1:T(8,128)(2,1)S(1)}, bf16[2048,128]{0,1:T(8,128)(2,1)}, u32[]{:S(2)}) copy-start(bf16[2048,128]{0,1:T(8,128)(2,1)} %copy-done.10) | copy-start | bytes 1572868
  159.0 4.5 %copy-start.9 = (bf16[2048,128]{0,1:T(8,128)(2,1)S(1)}, bf16[2048,128]{0,1:T(8,128)(2,1)}, u32[]{:S(2)}) copy-start(bf16[2048,128]{0,1:T(8,128)(2,1)} %copy-done.8) | copy-start | bytes 1572868
  251.5 103.9 %all-gather.2.cloned.1.call-start = ((), (), s32[]{:S(2)}) async-start(), calls=%async_computation.5 | async-start | bytes 9437184 | tf_op jit(solution)/shard_map/all_gather | solution.py:22
  326.6 5.2 %copy-start.17 = (bf16[1,128,16,128]{3,1,2,0:T(8,128)(2,1)S(1)}, bf16[1,128,16,128]{3,1,2,0:T(8,128)(2,1)}, u32[]{:S(2)}) copy-start(bf16[1,128,16,128]{3,1,2,0:T(8,128)(2,1)} %get-tuple-element.217) | copy-start | bytes 1572868
  327.9 34.7 %all-to-all-start.3 = ((bf16[16,32,1024]{2,1,0:T(8,128)(2,1)}), bf16[16,32,1024]{2,1,0:T(8,128)(2,1)S(1)}, u32[]{:S(2)}, u32[]{:S(2)}) async-start(bf16[16,32,1024]{2,1,0:T(8,128)(2,1)} %broadcast_in_dim.70), calls=%async_computation.4 | async-start | bytes 2097152 | tf_op jit(solution)/shard_map/all_to_all | solution.py:33
  (8 other events, 12.7 us)
Sparse Core Ops, SparseCore 0:
  251.6 51.1 reduce-scatter.1
  305.1 50.2 all-gather.1
where the time goes:
time: 373 us; the launch traced here: 371 us
  waiting for transfers between devices  102 us (27%)
  matrix products  69.1 us (19%)
  other arithmetic  63.2 us (17%)
  local copies, waits for them, and re-layouts  59.7 us (16%)
  blocking collectives  47.5 us (13%)
  between operations  14.4 us (4%)
  starting transfers between devices  12.4 us (3%)
    reduce_scatter x1, waiting for transfers between devices, on_device(): lax.psum_scatter(contract_rows(flat_in, kv_grad).astype(jnp.bfloat16), 'd...  49 us
    unnamed x3, other arithmetic  34.5 us
    all_to_all x1, waiting for transfers between devices, on_device(): lax.all_to_all(bundle, 'sp', split_axis=2, concat_axis=1, tiled=True)  30.8 us
    dot_general x9, matrix products, contract_rows(): lax.dot_general(left_side, right_side, (((0,), (0,)), ((), ())), preferre...  28.9 us
    unnamed x38, local copies, waits for them, and re-layouts  27.8 us
    all_to_all x1, blocking collectives, on_device(): lax.all_to_all(head_out, 'sp', split_axis=1, concat_axis=2, tiled=True)  25.3 us
    all_to_all x1, blocking collectives, sum_at_owner(): parts = lax.all_to_all(cut_along(array, dim, peers), axis, 0, 0, tiled=True)  22.3 us
    all_gather x1, waiting for transfers between devices, sent_together(): result = lax.all_gather(both, axis, axis=dim, tiled=True)  22.3 us
  transfers between devices with their start and end apart: 4, of which 3 were waited for; matrix products, arithmetic and copies ran while one was open for 3% of the time, Pallas kernels for 0%

commit v1 on v0

v1 whole, which is shorter than its diff:
```python
import functools

import jax
import jax.numpy as jnp
import numpy as np
from jax import lax
from jax.experimental import pallas as pl
from jax.experimental.pallas import tpu as pltpu
from jax.sharding import PartitionSpec as P

D = 128
GRID_W = 64
EPS = 1e-6
BASE = 10000.0
NZ = 4
NX = 4
NY = 4
NSP = NZ * NX
NDP = 2 * NY
T = 128
KC = 64
BF = jnp.bfloat16
F32 = jnp.float32
SCALE = D ** -0.5
EXP2_SCALE = float(SCALE * np.log2(np.e))


def rope_tables():
    quarter = D // 4
    inverse = np.float32(BASE) ** (-np.arange(quarter, dtype=np.float32) / np.float32(quarter))

    def one(count, half):
        angles = np.arange(count, dtype=np.float32)[:, None] * inverse[None, :]
        cosine, sine = np.cos(angles), np.sin(angles)
        table = np.zeros((3, count, D), np.float32)
        lo = half * 2 * quarter
        table[0, :, lo : lo + quarter] = cosine
        table[0, :, lo + quarter : lo + 2 * quarter] = cosine
        table[1, :, lo + quarter : lo + 2 * quarter] = sine
        table[2, :, lo : lo + quarter] = -sine
        return table

    rows = one(2048 // GRID_W, 0).reshape(3, 2048 // GRID_W, 1, D)
    cols = one(GRID_W, 1)
    return rows, cols


def rotate(n, c, s1, s2):
    return n * c + pltpu.roll(n, 32, 1) * s1 + pltpu.roll(n, 96, 1) * s2


def unrotate(n, c, s1, s2):
    return n * c - pltpu.roll(n, 32, 1) * s1 - pltpu.roll(n, 96, 1) * s2


def inv_rms(u):
    return lax.rsqrt(jnp.mean(u * u, axis=1, keepdims=True) + EPS)


def norm_back(grad, u, gain, c, s1, s2):
    r = inv_rms(u)
    t = unrotate(grad, c, s1, s2) * gain
    dot = jnp.sum(t * u, axis=1, keepdims=True)
    return r * t - u * (r * r * r * (1.0 / D) * dot)


def dot_nt(a, b):
    return lax.dot_general(a, b, (((1,), (1,)), ((), ())), preferred_element_type=F32)


def dot_nn(a, b):
    return lax.dot_general(a, b, (((1,), (0,)), ((), ())), preferred_element_type=F32)


def dot_tn(a, b):
    return lax.dot_general(a, b, (((0,), (0,)), ((), ())), preferred_element_type=F32)


def body(
    q, k, v, g, li, kw, vw, qg, kg, tr, tc,
    gq, gin, gw,
    q_all, g_all, k_all, v_all, k_src, k_t, tab, qs, gs, s_scr, dp_scr, pb, ds,
    dq_out, dv_src, dk_src, dv_in, dk_in, li_all, kw_s, vw_s, vs_all, ks_all,
    rs_src, rs_in, ag_src, gi_src,
    loc, zs, zr, xs, xr, lis, lir, dqs, dqr, dps, dpr, as_, ar, rss, rsr, ags, agr, gis, gir,
):
    sp = lax.axis_index("sp")
    dp = lax.axis_index("dp")
    z, x = sp // NX, lax.rem(sp, NX)
    y, core = dp // 2, lax.rem(dp, 2)

    def remote(src, dst, ss, rs, **where):
        return pltpu.make_async_remote_copy(
            src_ref=src, dst_ref=dst, send_sem=ss, recv_sem=rs,
            device_id=where, device_id_type=pl.DeviceIdType.MESH,
        )

    barrier = pltpu.get_barrier_semaphore()

    def greet_sp(o, _):
        pl.semaphore_signal(
            barrier, inc=1, device_id={"sp": lax.rem(sp + o, NSP)},
            device_id_type=pl.DeviceIdType.MESH,
        )
        return 0

    def greet_dp(o, _):
        pl.semaphore_signal(
            barrier, inc=1, device_id={"dp": lax.rem(dp + o, NDP)},
            device_id_type=pl.DeviceIdType.MESH,
        )
        return 0

    lax.fori_loop(1, NSP, greet_sp, 0)
    lax.fori_loop(1, NDP, greet_dp, 0)

    def cols(i, w):
        return pl.ds(pl.multiple_of(i * w, w), w)

    own = [
        pltpu.make_async_copy(q.at[:, cols(z, 512)], q_all.at[z], loc.at[0]),
        pltpu.make_async_copy(g.at[:, cols(z, 512)], g_all.at[z], loc.at[1]),
        pltpu.make_async_copy(v.at[:, cols(z, D)], v_all.at[x, z], loc.at[2]),
        pltpu.make_async_copy(li.at[:, cols(dp, 512)], li_all.at[dp], loc.at[3]),
        pltpu.make_async_copy(kw, kw_s, loc.at[4]),
        pltpu.make_async_copy(vw, vw_s, loc.at[5]),
    ]
    for c in own:
        c.start()

    for zz in range(NZ):
        shard = NX * zz + x
        for kind in range(3):
            part = tc[kind]
            tab[zz, kind, 0:64] = part + tr[kind, 2 * shard]
            tab[zz, kind, 64:128] = part + tr[kind, 2 * shard + 1]

    for h in range(NZ):
        u = k[:, h * D : (h + 1) * D].astype(F32)
        n = u * inv_rms(u) * kg[...]
        k_src[h] = rotate(n, tab[z, 0], tab[z, 1], tab[z, 2]).astype(BF)
    k_all[x, z] = k_src[z]

    pl.semaphore_wait(barrier, NSP + NDP - 2)

    def z_copies(o, side, kinds):
        peer = lax.rem(z + o, NZ)
        slot = z if side == "send" else peer
        pairs = (
            (k_src.at[peer], k_all.at[x, slot]),
            (v.at[:, cols(peer, D)], v_all.at[x, slot]),
            (q.at[:, cols(peer, 512)], q_all.at[slot]),
            (g.at[:, cols(peer, 512)], g_all.at[slot]),
        )
        return [
            remote(*pairs[i], zs.at[i, peer], zr.at[i, slot], sp=peer * NX + x) for i in kinds
        ]

    order = (1, 3, 2)
    for o in order:
        for c in z_copies(o, "send", (0, 1)):
            c.start()
    for o in order:
        for c in z_copies(o, "send", (2, 3)):
            c.start()

    def li_copy(o, side):
        peer = lax.rem(dp + o, NDP)
        slot = dp if side == "send" else peer
        return remote(li.at[:, cols(peer, 512)], li_all.at[slot], lis.at[peer], lir.at[slot], dp=peer)

    def li_start(o, _):
        li_copy(o, "send").start()
        return 0

    lax.fori_loop(1, NDP, li_start, 0)

    own[2].wait()
    for o in order:
        for c in z_copies(o, "recv", (0, 1)):
            c.wait_recv()

    def x_copies(o, side):
        peer = lax.rem(x + o, NX)
        slot = x if side == "send" else peer
        return [
            remote(k_all.at[slot], k_all.at[slot], xs.at[0, peer], xr.at[0, slot], sp=z * NX + peer),
            remote(v_all.at[slot], v_all.at[slot], xs.at[1, peer], xr.at[1, slot], sp=z * NX + peer),
        ]

    for o in order:
        for c in x_copies(o, "send"):
            c.start()
    own[0].wait()
    own[1].wait()
    for o in order:
        for c in x_copies(o, "recv"):
            c.wait_recv()
    k_t[...] = k_all[...].reshape(NSP * T, D).T

    def dq_copy(zz):
        return remote(dq_out.at[zz], gq.at[:, cols(z, 512)], dqs.at[zz], dqr.at[z], sp=zz * NX + x)

    def block(i, _):
        off = i // 2
        zz = lax.rem(z + off, NZ)
        pair = lax.rem(i, 2)

        @pl.when((pair == 0) & (off > 0))
        def _():
            remote(q.at[:, cols(z, 512)], q_all.at[zz], zs.at[2, zz], zr.at[2, zz], sp=zz * NX + x).wait_recv()
            remote(g.at[:, cols(z, 512)], g_all.at[zz], zs.at[3, zz], zr.at[3, zz], sp=zz * NX + x).wait_recv()

        c, s1, s2 = tab[zz, 0], tab[zz, 1], tab[zz, 2]
        wide = pl.ds(pl.multiple_of(pair * 256, 256), 256)
        rows = pl.ds(pl.multiple_of(i * 256, 256), 256)
        here = pl.ds(pl.multiple_of(i * 256, 256), 256)
        both = q_all[zz, :, wide].astype(F32)
        parts = []
        for h in range(2):
            u = both[:, h * D : (h + 1) * D]
            parts.append(rotate(u * inv_rms(u) * qg[...], c, s1, s2).astype(BF))
        qb = jnp.concatenate(parts, axis=0)
        qs[rows, :] = qb
        gb2 = g_all[zz, :, wide]
        gb = jnp.concatenate([gb2[:, :D], gb2[:, D:]], axis=0)
        gs[rows, :] = gb

        m8 = jnp.full((8, 256), -jnp.inf, F32)
        for j in range(8):
            kc = k_all[j // 2, 2 * (j % 2) : 2 * (j % 2) + 2].reshape(256, D)
            vc = v_all[j // 2, 2 * (j % 2) : 2 * (j % 2) + 2].reshape(256, D)
            s = dot_nt(kc, qb)
            s_scr[j * 256 : (j + 1) * 256, :] = s
            m8 = jnp.maximum(m8, jnp.max(s.reshape(32, 8, 256), axis=0))
            dp_scr[j * 256 : (j + 1) * 256, :] = dot_nt(vc, gb)
        m = jnp.max(m8, axis=0, keepdims=True)

        def exps(j, l8):
            at = pl.ds(pl.multiple_of(j * KC, KC), KC)
            e = jnp.exp2((s_scr[at, :] - m) * EXP2_SCALE)
            s_scr[at, :] = e
            return l8 + jnp.sum(e.reshape(KC // 8, 8, 256), axis=0)

        l8 = lax.fori_loop(0, 2048 // KC, exps, jnp.zeros((8, 256), F32), unroll=4)
        rl = 1.0 / jnp.sum(l8, axis=0, keepdims=True)

        def probs(j, d8):
            at = pl.ds(pl.multiple_of(j * KC, KC), KC)
            p = s_scr[at, :] * rl
            p_b = p.astype(BF)
            s_scr[at, :] = p
            pb[at, here] = p_b
            prod = p_b.astype(F32) * dp_scr[at, :]
            return d8 + jnp.sum(prod.reshape(KC // 8, 8, 256), axis=0)

        d8 = lax.fori_loop(0, 2048 // KC, probs, jnp.zeros((8, 256), F32), unroll=4)
        delta = jnp.sum(d8, axis=0, keepdims=True)

        def scores(j, _):
            at = pl.ds(pl.multiple_of(j * KC, KC), KC)
            ds[at, here] = (s_scr[at, :] * (dp_scr[at, :] - delta)).astype(BF)
            return 0

        lax.fori_loop(0, 2048 // KC, scores, 0, unroll=4)
        grad = dot_nn(k_t[...], ds[:, here]).T * SCALE
        outs = []
        for h in range(2):
            outs.append(
                norm_back(
                    grad[h * D : (h + 1) * D], both[:, h * D : (h + 1) * D], qg[...], c, s1, s2
                ).astype(BF)
            )
        dq_out[zz, :, wide] = jnp.concatenate(outs, axis=1)

        @pl.when(i == 1)
        def _():
            pltpu.make_async_copy(dq_out.at[z], gq.at[:, cols(z, 512)], loc.at[6]).start()

        @pl.when((pair == 1) & (off > 0))
        def _():
            dq_copy(zz).start()

        return 0

    lax.fori_loop(0, 8, block, 0)

    def grads_out(left, right, scale, src, into, which):
        def send(xx, zz):
            peer = zz * NX + xx
            return remote(
                src.at[xx, zz], into.at[sp], dps.at[which, peer], dpr.at[which, sp], sp=peer
            )

        def chunk(xx):
            at = pl.ds(pl.multiple_of(xx * 512, 512), 512)
            out = dot_nn(left[at, :], right[...])
            if scale is not None:
                out = out * scale
            src[xx] = out.astype(BF).reshape(NZ, T, D)

        def far(o, _):
            xx = lax.rem(x + o, NX)
            chunk(xx)
            for zz in range(NZ):
                send(xx, zz).start()
            return 0

        lax.fori_loop(1, NX, far, 0)
        chunk(x)
        for o in range(1, NZ):
            send(x, lax.rem(z + o, NZ)).start()
        into[sp] = src[x, z]

    grads_out(pb, gs, None, dv_src, dv_in, 0)
    grads_out(ds, qs, SCALE, dk_src, dk_in, 1)

    def wait_grads(src, into, which):
        def one(o, _):
            peer = lax.rem(sp + o, NSP)
            remote(src.at[0, 0], into.at[peer], dps.at[which, peer], dpr.at[which, peer], sp=peer).wait_recv()
            return 0

        lax.fori_loop(1, NSP, one, 0)

    def head_sum(into, h):
        total = into[NX * h].astype(F32)
        for xx in range(1, NX):
            total = total + into[NX * h + xx].astype(F32)
        return total

    def same(o, side, buf, which):
        peer = lax.rem(y + o, NY)
        slot = dp if side == "send" else 2 * peer + core
        return remote(buf.at[slot], buf.at[slot], as_.at[which, 2 * peer + core], ar.at[which, slot], dp=2 * peer + core)

    def cross(yy, side, buf, which):
        slot = 2 * yy + (core if side == "send" else 1 - core)
        return remote(buf.at[slot], buf.at[slot], as_.at[which + 2, yy], ar.at[which, slot], dp=2 * y + (1 - core))

    def gather_start(buf, which):
        for o in order:
            same(o, "send", buf, which).start()
        cross(y, "send", buf, which).start()

    def gather_finish(buf, which):
        for o in order:
            same(o, "recv", buf, which).wait_recv()
            cross(lax.rem(y + o, NY), "send", buf, which).start()
        for yy in range(NY):
            cross(yy, "recv", buf, which).wait_recv()

    wait_grads(dv_src, dv_in, 0)
    vs_all[dp] = jnp.concatenate([head_sum(dv_in, h).astype(BF) for h in range(NZ)], axis=1)
    gather_start(vs_all, 0)

    wait_grads(dk_src, dk_in, 1)
    pieces = []
    for h in range(NZ):
        u = k[:, h * D : (h + 1) * D].astype(F32)
        pieces.append(
            norm_back(head_sum(dk_in, h), u, kg[...], tab[z, 0], tab[z, 1], tab[z, 2]).astype(BF)
        )
    ks_all[dp] = jnp.concatenate(pieces, axis=1)
    gather_start(ks_all, 1)

    own[3].wait()

    def li_wait(o, _):
        li_copy(o, "recv").wait_recv()
        return 0

    lax.fori_loop(1, NDP, li_wait, 0)

    def reduce_start(buf, which):
        out = dot_tn(li_all[...].reshape(NDP * T, 512), buf[...].reshape(NDP * T, 512))
        rs_src[which] = out.astype(BF).reshape(NSP, 32, 512)
        rs_in[which, sp] = rs_src[which, sp]

        def one(o, _):
            peer = lax.rem(sp + o, NSP)
            remote(
                rs_src.at[which, peer], rs_in.at[which, sp], rss.at[which, peer], rsr.at[which, sp], sp=peer
            ).start()
            return 0

        lax.fori_loop(1, NSP, one, 0)

    def reduce_finish(which):
        def one(o, _):
            peer = lax.rem(sp + o, NSP)
            remote(
                rs_src.at[which, peer], rs_in.at[which, peer], rss.at[which, peer], rsr.at[which, peer], sp=peer
            ).wait_recv()
            return 0

        lax.fori_loop(1, NSP, one, 0)
        total = rs_in[which, 0].astype(F32)
        for i in range(1, NSP):
            total = total + rs_in[which, i].astype(F32)
        ag_src[which] = total.astype(BF)
        mine = pl.ds(pl.multiple_of(sp * 32, 32), 32)
        pltpu.make_async_copy(ag_src.at[which], gw.at[which, mine, :], loc.at[7 + which]).start()

        def two(o, _):
            peer = lax.rem(sp + o, NSP)
            remote(
                ag_src.at[which], gw.at[which, mine, :], ags.at[which, peer], agr.at[which, sp], sp=peer
            ).start()
            return 0

        lax.fori_loop(1, NSP, two, 0)

    gather_finish(vs_all, 0)
    reduce_start(vs_all, 0)
    gather_finish(ks_all, 1)
    reduce_start(ks_all, 1)

    own[4].wait()
    own[5].wait()

    def gi_copy(peer):
        return remote(gi_src.at[peer], gin.at[:, cols(dp, 512)], gis.at[peer], gir.at[dp], dp=peer)

    def grad_in(o, _):
        peer = lax.rem(dp + o, NDP)
        out = dot_nt(ks_all[peer], kw_s[...]) + dot_nt(vs_all[peer], vw_s[...])
        gi_src[peer] = out.astype(BF)

        @pl.when(o < NDP)
        def _():
            gi_copy(peer).start()

        return 0

    lax.fori_loop(1, NDP + 1, grad_in, 0)
    pltpu.make_async_copy(gi_src.at[dp], gin.at[:, cols(dp, 512)], loc.at[9]).start()

    reduce_finish(0)
    reduce_finish(1)

    pltpu.make_async_copy(dq_out.at[z], gq.at[:, cols(z, 512)], loc.at[6]).wait()
    pltpu.make_async_copy(gi_src.at[dp], gin.at[:, cols(dp, 512)], loc.at[9]).wait()
    mine = pl.ds(pl.multiple_of(sp * 32, 32), 32)
    for which in range(2):
        pltpu.make_async_copy(ag_src.at[which], gw.at[which, mine, :], loc.at[7 + which]).wait()
    for o in range(1, NZ):
        for c in z_copies(o, "send", (0, 1, 2, 3)):
            c.wait_send()
        for c in x_copies(o, "send"):
            c.wait_send()
        zz = lax.rem(z + o, NZ)
        dq_copy(zz).wait_send()
        remote(dq_out.at[zz], gq.at[:, cols(zz, 512)], dqs.at[zz], dqr.at[zz], sp=zz * NX + x).wait_recv()
    for which, buf in ((0, vs_all), (1, ks_all)):
        for o in range(1, NY):
            same(o, "send", buf, which).wait_send()
        for yy in range(NY):
            cross(yy, "send", buf, which).wait_send()

    def drain_dp(o, _):
        peer = lax.rem(dp + o, NDP)
        li_copy(o, "send").wait_send()
        gi_copy(peer).wait_send()
        remote(gi_src.at[peer], gin.at[:, cols(peer, 512)], gis.at[peer], gir.at[peer], dp=peer).wait_recv()
        return 0

    lax.fori_loop(1, NDP, drain_dp, 0)

    def drain_sp(o, _):
        peer = lax.rem(sp + o, NSP)
        theirs = pl.ds(pl.multiple_of(peer * 32, 32), 32)
        for which, src in ((0, dv_src), (1, dk_src)):
            remote(src.at[0, 0], dv_in.at[peer], dps.at[which, peer], dpr.at[which, peer], sp=peer).wait_send()
            remote(
                rs_src.at[which, peer], rs_in.at[which, peer], rss.at[which, peer], rsr.at[which, peer], sp=peer
            ).wait_send()
            c = remote(
                ag_src.at[which], gw.at[which, theirs, :], ags.at[which, peer], agr.at[which, peer], sp=peer
            )
            c.wait_send()
            c.wait_recv()
        return 0

    lax.fori_loop(1, NSP, drain_sp, 0)


def on_device(queries, keys, values, out_grad, layer_in, key_weight, value_weight, query_gain, key_gain):
    rows, cols = rope_tables()
    hbm = pl.BlockSpec(memory_space=pl.ANY)
    vmem = pl.BlockSpec(memory_space=pltpu.VMEM)
    dma = pltpu.SemaphoreType.DMA
    V = pltpu.VMEM
    gq, gin, gw = pl.pallas_call(
        body,
        out_shape=(
            jax.ShapeDtypeStruct((T, 2048), BF),
            jax.ShapeDtypeStruct((T, 4096), BF),
            jax.ShapeDtypeStruct((2, 512, 512), BF),
        ),
        in_specs=[hbm, vmem, hbm, hbm, hbm, hbm, hbm, vmem, vmem, vmem, vmem],
        out_specs=(hbm, hbm, hbm),
        scratch_shapes=[
            V((NZ, T, 512), BF),
            V((NZ, T, 512), BF),
            V((NX, NZ, T, D), BF),
            V((NX, NZ, T, D), BF),
            V((NZ, T, D), BF),
            V((D, 2048), BF),
            V((NZ, 3, T, D), F32),
            V((2048, D), BF),
            V((2048, D), BF),
            V((2048, 256), F32),
            V((2048, 256), F32),
            V((2048, 2048), BF),
            V((2048, 2048), BF),
            V((NZ, T, 512), BF),
            V((NX, NZ, T, D), BF),
            V((NX, NZ, T, D), BF),
            V((NSP, T, D), BF),
            V((NSP, T, D), BF),
            V((NDP, T, 512), BF),
            V((512, 512), BF),
            V((512, 512), BF),
            V((NDP, T, 512), BF),
            V((NDP, T, 512), BF),
            V((2, NSP, 32, 512), BF),
            V((2, NSP, 32, 512), BF),
            V((2, 32, 512), BF),
            V((NDP, T, 512), BF),
            dma((10,)),
            dma((4, NZ)),
            dma((4, NZ)),
            dma((2, NX)),
            dma((2, NX)),
            dma((NDP,)),
            dma((NDP,)),
            dma((NZ,)),
            dma((NZ,)),
            dma((2, NSP)),
            dma((2, NSP)),
            dma((4, NDP)),
            dma((2, NDP)),
            dma((2, NSP)),
            dma((2, NSP)),
            dma((2, NSP)),
            dma((2, NSP)),
            dma((NDP,)),
            dma((NDP,)),
        ],
        compiler_params=pltpu.CompilerParams(
            collective_id=0, has_side_effects=True, vmem_limit_bytes=60 * 1024 * 1024
        ),
        name="step",
    )(
        queries[0], keys[0], values[0], out_grad[0], layer_in[0], key_weight, value_weight,
        query_gain.reshape(1, D), key_gain.reshape(1, D), jnp.asarray(rows), jnp.asarray(cols),
    )
    return gq[None], gin[None], gw[1].astype(F32), gw[0].astype(F32)


def solution(mesh):
    in_specs = (
        P("dp", "sp", None),
        P("dp", "sp", None),
        P("dp", "sp", None),
        P("dp", "sp", None),
        P("dp", "sp", None),
        P("dp", None),
        P("dp", None),
        P(),
        P(),
    )
    out_specs = (P("dp", "sp", None), P("dp", "sp", None), P("dp", None), P("dp", None))
    return jax.shard_map(
        on_device, mesh=mesh, in_specs=in_specs, out_specs=out_specs, check_vma=False
    )
```

time: 373 us -> 110 us (0.29)
  Pallas kernels: 0 us -> 104 us
  waiting for transfers between devices: 102 us -> 0 us
  matrix products: 69.1 us -> 0 us
  other arithmetic: 63.2 us -> 2.86 us
  local copies, waits for them, and re-layouts: 59.7 us -> 2.38 us
  blocking collectives: 47.5 us -> 0 us
  between operations: 14.4 us -> 0.65 us
  starting transfers between devices: 12.4 us -> 0 us
    pallas_call x0 -> x1, Pallas kernels: none -> 104 us  [on_device(): pl.pallas_call(body, out_shape=(jax.ShapeDtypeStruct((T, 2048), BF), jax....]
    dot_general x26 -> x0, matrix products: 69.1 us -> none  [the longest x9 28.9 us: contract_rows(): lax.dot_general(left_side, right_side, (((0,), (0,)), ((), ())), preferre...]
    reduce_scatter x1 -> x0, waiting for transfers between devices: 49 us -> none  [on_device(): lax.psum_scatter(contract_rows(flat_in, kv_grad).astype(jnp.bfloat16), 'd...]
    all_to_all x2 -> x0, blocking collectives: 47.5 us -> none  [the longest x1 25.3 us: on_device(): lax.all_to_all(head_out, 'sp', split_axis=1, concat_axis=2, tiled=True)]
    unnamed x3 -> x0, other arithmetic: 34.5 us -> none
    all_to_all x2 -> x0, waiting for transfers between devices: 30.8 us -> none  [the longest x1 30.8 us: on_device(): lax.all_to_all(bundle, 'sp', split_axis=2, concat_axis=1, tiled=True)]
    unnamed x38 -> x6, local copies, waits for them, and re-layouts: 27.8 us -> 2.38 us
    all_gather x1 -> x0, waiting for transfers between devices: 22.3 us -> none  [sent_together(): result = lax.all_gather(both, axis, axis=dim, tiled=True)]
  transfers between devices with their start and end apart: 4 -> 0, of which waited for: 3 -> 0; matrix products, arithmetic and copies ran while one was open for 3% -> 0% of each run, Pallas kernels for 0% -> 0%
where the time goes in v1:
time: 110 us
  Pallas kernels  104 us (95%)
  other arithmetic  2.86 us (3%)
  local copies, waits for them, and re-layouts  2.38 us (2%)
    pallas_call x1, Pallas kernels, on_device(): pl.pallas_call(body, out_shape=(jax.ShapeDtypeStruct((T, 2048), BF), jax....  104 us
    convert_element_type x1, other arithmetic, on_device(): return (gq[None], gin[None], gw[1].astype(F32), gw[0].astype(F32))  2.86 us
    unnamed x6, local copies, waits for them, and re-layouts  2.38 us

profile of v1, /device:TPU:1, one launch (start us, length us, event | category | flops | bytes accessed | tf_op | source)
XLA Modules:
  0.0 110.1 jit_solution(14412411004473472823)
XLA Ops:
  0.6 104.2 %step.1 = (bf16[128,2048]{1,0:T(8,128)(2,1)}, bf16[128,4096]{1,0:T(8,128)(2,1)}, bf16[2,512,512]{2,1,0:T(8,128)(2,1)}) custom-call(bf16[128,2048]{1,0:T(8,128)(2,1)} %bitcast.18, bf16[128,512]{1,0:T(8,128)(2,1)} %bitcast.20, bf16[128,512]{1,0:T(8,128)(2,1)} %bitcast.21, bf16[128,2048]{1,0:T(8,128)(2,1)} %bitcast.19, bf16[128,4096]{1,0:T(8,128)(2,1)} %bitcast.16, ...), custom_call_target="tpu_custom_call" | custom-call | tf_op jit(solution)/shard_map/step/pallas_call | solution.py:494
  104.9 0.0 copy-start.1
  104.9 2.9 %bitcast_convert_fusion = (f32[512,512]{1,0:T(8,128)}, f32[512,512]{1,0:T(8,128)}) fusion(bf16[2,512,512]{2,1,0:T(8,128)(2,1)} %get-tuple-element.9), kind=kLoop, calls=%fused_computation | loop fusion | flops 524288 | bytes 3145728 | tf_op jit(solution)/shard_map/convert_element_type | solution.py:559
  107.8 0.0 copy-start
  107.8 0.0 copy-done.1
  107.8 0.8 copy.17
  108.6 0.6 copy-done
  109.2 1.0 copy.18
Async XLA Ops:
  104.9 2.9 %copy-start.1 = (bf16[128,2048]{1,0:T(8,128)(2,1)S(1)}, bf16[128,2048]{1,0:T(8,128)(2,1)}, u32[]{:S(2)}) copy-start(bf16[128,2048]{1,0:T(8,128)(2,1)} %get-tuple-element.7) | copy-start | bytes 1572868
  107.8 1.4 %copy-start = (bf16[128,4096]{1,0:T(8,128)(2,1)S(1)}, bf16[128,4096]{1,0:T(8,128)(2,1)}, u32[]{:S(2)}) copy-start(bf16[128,4096]{1,0:T(8,128)(2,1)} %get-tuple-element.8) | copy-start | bytes 3145732

commit v2 on v1

--- a/solution.py
+++ b/solution.py
@@ -79,7 +79,7 @@
 def body(
     q, k, v, g, li, kw, vw, qg, kg, tr, tc,
     gq, gin, gw,
-    q_all, g_all, k_all, v_all, k_src, k_t, tab, qs, gs, s_scr, dp_scr, pb, ds,
+    q_all, g_all, k_all, v_all, k_src, k_t, tab, qs, gs, m_scr, s_all, dp_all, pb,
     dq_out, dv_src, dk_src, dv_in, dk_in, li_all, kw_s, vw_s, vs_all, ks_all,
     rs_src, rs_in, ag_src, gi_src,
     loc, zs, zr, xs, xr, lis, lir, dqs, dqr, dps, dpr, as_, ar, rss, rsr, ags, agr, gis, gir,
@@ -141,7 +141,8 @@
         k_src[h] = rotate(n, tab[z, 0], tab[z, 1], tab[z, 2]).astype(BF)
     k_all[x, z] = k_src[z]
 
-    pl.semaphore_wait(barrier, NSP + NDP - 2)
+    with jax.named_scope("s_barrier"):
+        pl.semaphore_wait(barrier, NSP + NDP - 2)
 
     def z_copies(o, side, kinds):
         peer = lax.rem(z + o, NZ)
@@ -176,9 +177,10 @@
     lax.fori_loop(1, NDP, li_start, 0)
 
     own[2].wait()
-    for o in order:
-        for c in z_copies(o, "recv", (0, 1)):
-            c.wait_recv()
+    with jax.named_scope("s_zkv"):
+        for o in order:
+            for c in z_copies(o, "recv", (0, 1)):
+                c.wait_recv()
 
     def x_copies(o, side):
         peer = lax.rem(x + o, NX)
@@ -191,99 +193,102 @@
     for o in order:
         for c in x_copies(o, "send"):
             c.start()
+
+    def dq_copy(zz):
+        return remote(dq_out.at[zz], gq.at[:, cols(z, 512)], dqs.at[zz], dqr.at[z], sp=zz * NX + x)
+
+    def prepare(o):
+        zz = lax.rem(z + o, NZ)
+        for h in range(4):
+            rows = pl.ds(pl.multiple_of(o * 512 + h * T, T), T)
+            u = q_all[zz, :, h * D : (h + 1) * D].astype(F32)
+            n = u * inv_rms(u) * qg[...]
+            qs[rows, :] = rotate(n, tab[zz, 0], tab[zz, 1], tab[zz, 2]).astype(BF)
+            gs[rows, :] = g_all[zz, :, h * D : (h + 1) * D]
+
+    def unit(xo, o):
+        xx = lax.rem(x + xo, NX)
+        qcols = pl.ds(pl.multiple_of(o * 512, 512), 512)
+        qb, gb = qs[qcols, :], gs[qcols, :]
+        for half in range(2):
+            kc = k_all[xx, 2 * half : 2 * half + 2].reshape(256, D)
+            vc = v_all[xx, 2 * half : 2 * half + 2].reshape(256, D)
+            rows = pl.ds(pl.multiple_of(xx * 512 + half * 256, 256), 256)
+            s = dot_nt(kc, qb)
+            s_all[rows, qcols] = s
+            m_scr[:, qcols] = jnp.maximum(m_scr[:, qcols], jnp.max(s.reshape(32, 8, 512), axis=0))
+            dp_all[rows, qcols] = dot_nt(vc, gb)
+
+    def wait_x(o):
+        for c in x_copies(o, "recv"):
+            c.wait_recv()
+
+    def wait_q(o):
+        for c in z_copies(o, "recv", (2, 3)):
+            c.wait_recv()
+
+    def three(i):
+        return i + i // 2
+
+    m_scr[...] = jnp.full((8, 2048), -jnp.inf, F32)
     own[0].wait()
     own[1].wait()
-    for o in order:
-        for c in x_copies(o, "recv"):
-            c.wait_recv()
-    k_t[...] = k_all[...].reshape(NSP * T, D).T
-
-    def dq_copy(zz):
-        return remote(dq_out.at[zz], gq.at[:, cols(z, 512)], dqs.at[zz], dqr.at[z], sp=zz * NX + x)
-
-    def block(i, _):
-        off = i // 2
-        zz = lax.rem(z + off, NZ)
-        pair = lax.rem(i, 2)
-
-        @pl.when((pair == 0) & (off > 0))
-        def _():
-            remote(q.at[:, cols(z, 512)], q_all.at[zz], zs.at[2, zz], zr.at[2, zz], sp=zz * NX + x).wait_recv()
-            remote(g.at[:, cols(z, 512)], g_all.at[zz], zs.at[3, zz], zr.at[3, zz], sp=zz * NX + x).wait_recv()
-
-        c, s1, s2 = tab[zz, 0], tab[zz, 1], tab[zz, 2]
-        wide = pl.ds(pl.multiple_of(pair * 256, 256), 256)
-        rows = pl.ds(pl.multiple_of(i * 256, 256), 256)
+    with jax.named_scope("s_u0"):
+        prepare(0)
+        unit(0, 0)
+
+    def near_keys(i, _):
+        o = 1 + 2 * i
+        wait_x(o)
+        unit(o, 0)
+        return 0
+
+    with jax.named_scope("s_u1"):
+        lax.fori_loop(0, 2, near_keys, 0)
+
+    def near_queries(i, _):
+        o = 1 + 2 * i
+        wait_q(o)
+        prepare(o)
+        lax.fori_loop(0, 3, lambda j, _: (unit(three(j), o), 0)[1], 0)
+        return 0
+
+    with jax.named_scope("s_u2"):
+        lax.fori_loop(0, 2, near_queries, 0)
+    with jax.named_scope("s_u3"):
+        wait_x(2)
+        lax.fori_loop(0, 3, lambda j, _: (unit(2, three(j)), 0)[1], 0)
+    with jax.named_scope("s_u4"):
+        wait_q(2)
+        prepare(2)
+        lax.fori_loop(0, 4, lambda j, _: (unit(j, 2), 0)[1], 0)
+        k_t[...] = k_all[...].reshape(NSP * T, D).T
+
+    def soft(i, _):
         here = pl.ds(pl.multiple_of(i * 256, 256), 256)
-        both = q_all[zz, :, wide].astype(F32)
-        parts = []
-        for h in range(2):
-            u = both[:, h * D : (h + 1) * D]
-            parts.append(rotate(u * inv_rms(u) * qg[...], c, s1, s2).astype(BF))
-        qb = jnp.concatenate(parts, axis=0)
-        qs[rows, :] = qb
-        gb2 = g_all[zz, :, wide]
-        gb = jnp.concatenate([gb2[:, :D], gb2[:, D:]], axis=0)
-        gs[rows, :] = gb
-
-        m8 = jnp.full((8, 256), -jnp.inf, F32)
-        for j in range(8):
-            kc = k_all[j // 2, 2 * (j % 2) : 2 * (j % 2) + 2].reshape(256, D)
-            vc = v_all[j // 2, 2 * (j % 2) : 2 * (j % 2) + 2].reshape(256, D)
-            s = dot_nt(kc, qb)
-            s_scr[j * 256 : (j + 1) * 256, :] = s
-            m8 = jnp.maximum(m8, jnp.max(s.reshape(32, 8, 256), axis=0))
-            dp_scr[j * 256 : (j + 1) * 256, :] = dot_nt(vc, gb)
-        m = jnp.max(m8, axis=0, keepdims=True)
+        m = jnp.max(m_scr[:, here], axis=0, keepdims=True) * EXP2_SCALE
 
         def exps(j, l8):
             at = pl.ds(pl.multiple_of(j * KC, KC), KC)
-            e = jnp.exp2((s_scr[at, :] - m) * EXP2_SCALE)
-            s_scr[at, :] = e
+            e = jnp.exp2(s_all[at, here] * EXP2_SCALE - m)
+            s_all[at, here] = e
             return l8 + jnp.sum(e.reshape(KC // 8, 8, 256), axis=0)
 
         l8 = lax.fori_loop(0, 2048 // KC, exps, jnp.zeros((8, 256), F32), unroll=4)
         rl = 1.0 / jnp.sum(l8, axis=0, keepdims=True)
 
-        def probs(j, d8):
+        def probs(j, _):
             at = pl.ds(pl.multiple_of(j * KC, KC), KC)
-            p = s_scr[at, :] * rl
-            p_b = p.astype(BF)
-            s_scr[at, :] = p
-            pb[at, here] = p_b
-            prod = p_b.astype(F32) * dp_scr[at, :]
-            return d8 + jnp.sum(prod.reshape(KC // 8, 8, 256), axis=0)
-
-        d8 = lax.fori_loop(0, 2048 // KC, probs, jnp.zeros((8, 256), F32), unroll=4)
-        delta = jnp.sum(d8, axis=0, keepdims=True)
-
-        def scores(j, _):
-            at = pl.ds(pl.multiple_of(j * KC, KC), KC)
-            ds[at, here] = (s_scr[at, :] * (dp_scr[at, :] - delta)).astype(BF)
+            p = s_all[at, here] * rl
+            s_all[at, here] = p
+            pb[at, here] = p.astype(BF)
             return 0
 
-        lax.fori_loop(0, 2048 // KC, scores, 0, unroll=4)
-        grad = dot_nn(k_t[...], ds[:, here]).T * SCALE
-        outs = []
-        for h in range(2):
-            outs.append(
-                norm_back(
-                    grad[h * D : (h + 1) * D], both[:, h * D : (h + 1) * D], qg[...], c, s1, s2
-                ).astype(BF)
-            )
-        dq_out[zz, :, wide] = jnp.concatenate(outs, axis=1)
-
-        @pl.when(i == 1)
-        def _():
-            pltpu.make_async_copy(dq_out.at[z], gq.at[:, cols(z, 512)], loc.at[6]).start()
-
-        @pl.when((pair == 1) & (off > 0))
-        def _():
-            dq_copy(zz).start()
-
-        return 0
-
-    lax.fori_loop(0, 8, block, 0)
+        lax.fori_loop(0, 2048 // KC, probs, 0, unroll=4)
+        return 0
+
+    with jax.named_scope("s_soft"):
+        lax.fori_loop(0, 8, soft, 0)
 
     def grads_out(left, right, scale, src, into, which):
         def send(xx, zz):
@@ -312,9 +317,6 @@
             send(x, lax.rem(z + o, NZ)).start()
         into[sp] = src[x, z]
 
-    grads_out(pb, gs, None, dv_src, dv_in, 0)
-    grads_out(ds, qs, SCALE, dk_src, dk_in, 1)
-
     def wait_grads(src, into, which):
         def one(o, _):
             peer = lax.rem(sp + o, NSP)
@@ -350,11 +352,116 @@
         for yy in range(NY):
             cross(yy, "recv", buf, which).wait_recv()
 
-    wait_grads(dv_src, dv_in, 0)
+    def reduce_start(buf, which):
+        out = dot_tn(li_all[...].reshape(NDP * T, 512), buf[...].reshape(NDP * T, 512))
+        rs_src[which] = out.astype(BF).reshape(NSP, 32, 512)
+        rs_in[which, sp] = rs_src[which, sp]
+
+        def one(o, _):
+            peer = lax.rem(sp + o, NSP)
+            remote(
+                rs_src.at[which, peer], rs_in.at[which, sp], rss.at[which, peer], rsr.at[which, sp], sp=peer
+            ).start()
+            return 0
+
+        lax.fori_loop(1, NSP, one, 0)
+
+    def reduce_finish(which):
+        def one(o, _):
+            peer = lax.rem(sp + o, NSP)
+            remote(
+                rs_src.at[which, peer], rs_in.at[which, peer], rss.at[which, peer], rsr.at[which, peer], sp=peer
+            ).wait_recv()
+            return 0
+
+        lax.fori_loop(1, NSP, one, 0)
+        total = rs_in[which, 0].astype(F32)
+        for i in range(1, NSP):
+            total = total + rs_in[which, i].astype(F32)
+        ag_src[which] = total.astype(BF)
+        mine = pl.ds(pl.multiple_of(sp * 32, 32), 32)
+        pltpu.make_async_copy(ag_src.at[which], gw.at[which, mine, :], loc.at[7 + which]).start()
+
+        def two(o, _):
+            peer = lax.rem(sp + o, NSP)
+            remote(
+                ag_src.at[which], gw.at[which, mine, :], ags.at[which, peer], agr.at[which, sp], sp=peer
+            ).start()
+            return 0
+
+        lax.fori_loop(1, NSP, two, 0)
+
+    with jax.named_scope("s_dv"):
+        grads_out(pb, gs, None, dv_src, dv_in, 0)
+
+    def back(i, _):
+        off = i // 2
+        zz = lax.rem(z + off, NZ)
+        pair = lax.rem(i, 2)
+        here = pl.ds(pl.multiple_of(i * 256, 256), 256)
+        wide = pl.ds(pl.multiple_of(pair * 256, 256), 256)
+
+        def deltas(j, d8):
+            at = pl.ds(pl.multiple_of(j * KC, KC), KC)
+            prod = pb[at, here].astype(F32) * dp_all[at, here]
+            return d8 + jnp.sum(prod.reshape(KC // 8, 8, 256), axis=0)
+
+        d8 = lax.fori_loop(0, 2048 // KC, deltas, jnp.zeros((8, 256), F32), unroll=4)
+        delta = jnp.sum(d8, axis=0, keepdims=True)
+
+        def scores(j, _):
+            at = pl.ds(pl.multiple_of(j * KC, KC), KC)
+            pb[at, here] = (s_all[at, here] * (dp_all[at, here] - delta)).astype(BF)
+            return 0
+
+        lax.fori_loop(0, 2048 // KC, scores, 0, unroll=4)
+        grad = dot_nn(k_t[...], pb[:, here]).T * SCALE
+        both = q_all[zz, :, wide].astype(F32)
+        outs = []
+        for h in range(2):
+            outs.append(
+                norm_back(
+                    grad[h * D : (h + 1) * D], both[:, h * D : (h + 1) * D], qg[...],
+                    tab[zz, 0], tab[zz, 1], tab[zz, 2],
+                ).astype(BF)
+            )
+        dq_out[zz, :, wide] = jnp.concatenate(outs, axis=1)
+
+        @pl.when(i == 1)
+        def _():
+            pltpu.make_async_copy(dq_out.at[z], gq.at[:, cols(z, 512)], loc.at[6]).start()
+
+        @pl.when((pair == 1) & (off > 0))
+        def _():
+            dq_copy(zz).start()
+
+        return 0
+
+    with jax.named_scope("s_back"):
+        lax.fori_loop(0, 8, back, 0)
+
+    with jax.named_scope("s_wdv"):
+        wait_grads(dv_src, dv_in, 0)
     vs_all[dp] = jnp.concatenate([head_sum(dv_in, h).astype(BF) for h in range(NZ)], axis=1)
     gather_start(vs_all, 0)
-
-    wait_grads(dk_src, dk_in, 1)
+    with jax.named_scope("s_dk"):
+        grads_out(pb, qs, SCALE, dk_src, dk_in, 1)
+
+    own[3].wait()
+
+    def li_wait(o, _):
+        li_copy(o, "recv").wait_recv()
+        return 0
+
+    lax.fori_loop(1, NDP, li_wait, 0)
+
+    with jax.named_scope("s_gfv"):
+        gather_finish(vs_all, 0)
+    with jax.named_scope("s_rsv"):
+        reduce_start(vs_all, 0)
+
+    with jax.named_scope("s_wdk"):
+        wait_grads(dk_src, dk_in, 1)
     pieces = []
     for h in range(NZ):
         u = k[:, h * D : (h + 1) * D].astype(F32)
@@ -364,57 +471,12 @@
     ks_all[dp] = jnp.concatenate(pieces, axis=1)
     gather_start(ks_all, 1)
 
-    own[3].wait()
-
-    def li_wait(o, _):
-        li_copy(o, "recv").wait_recv()
-        return 0
-
-    lax.fori_loop(1, NDP, li_wait, 0)
-
-    def reduce_start(buf, which):
-        out = dot_tn(li_all[...].reshape(NDP * T, 512), buf[...].reshape(NDP * T, 512))
-        rs_src[which] = out.astype(BF).reshape(NSP, 32, 512)
-        rs_in[which, sp] = rs_src[which, sp]
-
-        def one(o, _):
-            peer = lax.rem(sp + o, NSP)
-            remote(
-                rs_src.at[which, peer], rs_in.at[which, sp], rss.at[which, peer], rsr.at[which, sp], sp=peer
-            ).start()
-            return 0
-
-        lax.fori_loop(1, NSP, one, 0)
-
-    def reduce_finish(which):
-        def one(o, _):
-            peer = lax.rem(sp + o, NSP)
-            remote(
-                rs_src.at[which, peer], rs_in.at[which, peer], rss.at[which, peer], rsr.at[which, peer], sp=peer
-            ).wait_recv()
-            return 0
-
-        lax.fori_loop(1, NSP, one, 0)
-        total = rs_in[which, 0].astype(F32)
-        for i in range(1, NSP):
-            total = total + rs_in[which, i].astype(F32)
-        ag_src[which] = total.astype(BF)
-        mine = pl.ds(pl.multiple_of(sp * 32, 32), 32)
-        pltpu.make_async_copy(ag_src.at[which], gw.at[which, mine, :], loc.at[7 + which]).start()
-
-        def two(o, _):
-            peer = lax.rem(sp + o, NSP)
-            remote(
-                ag_src.at[which], gw.at[which, mine, :], ags.at[which, peer], agr.at[which, sp], sp=peer
-            ).start()
-            return 0
-
-        lax.fori_loop(1, NSP, two, 0)
-
-    gather_finish(vs_all, 0)
-    reduce_start(vs_all, 0)
-    gather_finish(ks_all, 1)
-    reduce_start(ks_all, 1)
+    with jax.named_scope("s_rfv"):
+        reduce_finish(0)
+    with jax.named_scope("s_gfk"):
+        gather_finish(ks_all, 1)
+    with jax.named_scope("s_rsk"):
+        reduce_start(ks_all, 1)
 
     own[4].wait()
     own[5].wait()
@@ -433,11 +495,12 @@
 
         return 0
 
-    lax.fori_loop(1, NDP + 1, grad_in, 0)
+    with jax.named_scope("s_gin"):
+        lax.fori_loop(1, NDP + 1, grad_in, 0)
     pltpu.make_async_copy(gi_src.at[dp], gin.at[:, cols(dp, 512)], loc.at[9]).start()
 
-    reduce_finish(0)
-    reduce_finish(1)
+    with jax.named_scope("s_rfk"):
+        reduce_finish(1)
 
     pltpu.make_async_copy(dq_out.at[z], gq.at[:, cols(z, 512)], loc.at[6]).wait()
     pltpu.make_async_copy(gi_src.at[dp], gin.at[:, cols(dp, 512)], loc.at[9]).wait()
@@ -465,7 +528,8 @@
         remote(gi_src.at[peer], gin.at[:, cols(peer, 512)], gis.at[peer], gir.at[peer], dp=peer).wait_recv()
         return 0
 
-    lax.fori_loop(1, NDP, drain_dp, 0)
+    with jax.named_scope("s_drdp"):
+        lax.fori_loop(1, NDP, drain_dp, 0)
 
     def drain_sp(o, _):
         peer = lax.rem(sp + o, NSP)
@@ -482,7 +546,8 @@
             c.wait_recv()
         return 0
 
-    lax.fori_loop(1, NSP, drain_sp, 0)
+    with jax.named_scope("s_drsp"):
+        lax.fori_loop(1, NSP, drain_sp, 0)
 
 
 def on_device(queries, keys, values, out_grad, layer_in, key_weight, value_weight, query_gain, key_gain):
@@ -510,9 +575,9 @@
             V((NZ, 3, T, D), F32),
             V((2048, D), BF),
             V((2048, D), BF),
-            V((2048, 256), F32),
-            V((2048, 256), F32),
-            V((2048, 2048), BF),
+            V((8, 2048), F32),
+            V((2048, 2048), F32),
+            V((2048, 2048), F32),
             V((2048, 2048), BF),
             V((NZ, T, 512), BF),
             V((NX, NZ, T, D), BF),
@@ -549,7 +614,7 @@
             dma((NDP,)),
         ],
         compiler_params=pltpu.CompilerParams(
-            collective_id=0, has_side_effects=True, vmem_limit_bytes=60 * 1024 * 1024
+            collective_id=0, has_side_effects=True, vmem_limit_bytes=63 * 1024 * 1024
         ),
         name="step",
     )(

time: 110 us -> 102 us (0.927)
  Pallas kernels: 104 us -> 96.4 us
    pallas_call x1, Pallas kernels: 104 us -> 96.4 us  [on_device(): pl.pallas_call(body, out_shape=(jax.ShapeDtypeStruct((T, 2048), BF), jax....]
where the time goes in v2:
time: 102 us
  Pallas kernels  96.4 us (95%)
  other arithmetic  2.86 us (3%)
  local copies, waits for them, and re-layouts  2.38 us (2%)
    pallas_call x1, Pallas kernels, on_device(): pl.pallas_call(body, out_shape=(jax.ShapeDtypeStruct((T, 2048), BF), jax....  96.4 us
    convert_element_type x1, other arithmetic, on_device(): return (gq[None], gin[None], gw[1].astype(F32), gw[0].astype(F32))  2.86 us
    unnamed x6, local copies, waits for them, and re-layouts  2.38 us

profile of v2, /device:TPU:1, one launch (start us, length us, event | category | flops | bytes accessed | tf_op | source)
XLA Modules:
  0.0 102.3 jit_solution(7986771476607592935)
XLA Ops:
  0.6 96.4 %step.1 = (bf16[128,2048]{1,0:T(8,128)(2,1)}, bf16[128,4096]{1,0:T(8,128)(2,1)}, bf16[2,512,512]{2,1,0:T(8,128)(2,1)}) custom-call(bf16[128,2048]{1,0:T(8,128)(2,1)} %bitcast.18, bf16[128,512]{1,0:T(8,128)(2,1)} %bitcast.20, bf16[128,512]{1,0:T(8,128)(2,1)} %bitcast.21, bf16[128,2048]{1,0:T(8,128)(2,1)} %bitcast.19, bf16[128,4096]{1,0:T(8,128)(2,1)} %bitcast.16, ...), custom_call_target="tpu_custom_call" | custom-call | tf_op jit(solution)/shard_map/step/pallas_call | solution.py:559
  97.0 0.0 copy-start.1
  97.0 2.9 %bitcast_convert_fusion = (f32[512,512]{1,0:T(8,128)}, f32[512,512]{1,0:T(8,128)}) fusion(bf16[2,512,512]{2,1,0:T(8,128)(2,1)} %get-tuple-element.9), kind=kLoop, calls=%fused_computation | loop fusion | flops 524288 | bytes 3145728 | tf_op jit(solution)/shard_map/convert_element_type | solution.py:624
  99.9 0.0 copy-start
  99.9 0.0 copy-done.1
  99.9 0.8 copy.17
  100.7 0.6 copy-done
  101.3 1.0 copy.18
Async XLA Ops:
  97.0 2.9 %copy-start.1 = (bf16[128,2048]{1,0:T(8,128)(2,1)S(1)}, bf16[128,2048]{1,0:T(8,128)(2,1)}, u32[]{:S(2)}) copy-start(bf16[128,2048]{1,0:T(8,128)(2,1)} %get-tuple-element.7) | copy-start | bytes 1572868
  99.9 1.4 %copy-start = (bf16[128,4096]{1,0:T(8,128)(2,1)S(1)}, bf16[128,4096]{1,0:T(8,128)(2,1)}, u32[]{:S(2)}) copy-start(bf16[128,4096]{1,0:T(8,128)(2,1)} %get-tuple-element.8) | copy-start | bytes 3145732

commit v3 on v2

v3 whole, which is shorter than its diff:
```python
import functools

import jax
import jax.numpy as jnp
import numpy as np
from jax import lax
from jax.experimental import pallas as pl
from jax.experimental.pallas import tpu as pltpu
from jax.sharding import PartitionSpec as P

D = 128
GRID_W = 64
EPS = 1e-6
BASE = 10000.0
NZ = 4
NX = 4
NY = 4
NSP = NZ * NX
NDP = 2 * NY
T = 128
KC = 64
BF = jnp.bfloat16
F32 = jnp.float32
SCALE = D ** -0.5
EXP2_SCALE = float(SCALE * np.log2(np.e))


def rope_tables():
    quarter = D // 4
    inverse = np.float32(BASE) ** (-np.arange(quarter, dtype=np.float32) / np.float32(quarter))

    def one(count, half):
        angles = np.arange(count, dtype=np.float32)[:, None] * inverse[None, :]
        cosine, sine = np.cos(angles), np.sin(angles)
        table = np.zeros((3, count, D), np.float32)
        lo = half * 2 * quarter
        table[0, :, lo : lo + quarter] = cosine
        table[0, :, lo + quarter : lo + 2 * quarter] = cosine
        table[1, :, lo + quarter : lo + 2 * quarter] = sine
        table[2, :, lo : lo + quarter] = -sine
        return table

    rows = one(2048 // GRID_W, 0).reshape(3, 2048 // GRID_W, 1, D)
    cols = one(GRID_W, 1)
    return rows, cols


def rotate(n, c, s1, s2):
    return n * c + pltpu.roll(n, 32, 1) * s1 + pltpu.roll(n, 96, 1) * s2


def unrotate(n, c, s1, s2):
    return n * c - pltpu.roll(n, 32, 1) * s1 - pltpu.roll(n, 96, 1) * s2


def inv_rms(u):
    return lax.rsqrt(jnp.mean(u * u, axis=1, keepdims=True) + EPS)


def norm_back(grad, u, gain, c, s1, s2):
    r = inv_rms(u)
    t = unrotate(grad, c, s1, s2) * gain
    dot = jnp.sum(t * u, axis=1, keepdims=True)
    return r * t - u * (r * r * r * (1.0 / D) * dot)


def dot_nt(a, b):
    return lax.dot_general(a, b, (((1,), (1,)), ((), ())), preferred_element_type=F32)


def dot_nn(a, b):
    return lax.dot_general(a, b, (((1,), (0,)), ((), ())), preferred_element_type=F32)


def dot_tn(a, b):
    return lax.dot_general(a, b, (((0,), (0,)), ((), ())), preferred_element_type=F32)


def body(
    q, k, v, g, li, kw, vw, qg, kg, tr, tc,
    gq, gin, gwv, gwk,
    q_all, g_all, k_all, v_all, k_src, k_t, tab, qs, gs, m_scr, rl_scr, d_scr, s_all, dp_all, pb, ds,
    dq_out, dv_src, dk_src, dv_in, dk_in, li_all, kw_s, vw_s, vs_all, ks_all,
    r1, st1, r2, go,
    loc, zs, zr, xs, xr, lis, lir, dqs, dqr, dps, dpr, as_, ar, ts, tr_, gis, gir,
):
    sp = lax.axis_index("sp")
    dp = lax.axis_index("dp")
    z, x = sp // NX, lax.rem(sp, NX)
    y, core = dp // 2, lax.rem(dp, 2)

    def remote(src, dst, ss, rs, **where):
        return pltpu.make_async_remote_copy(
            src_ref=src, dst_ref=dst, send_sem=ss, recv_sem=rs,
            device_id=where, device_id_type=pl.DeviceIdType.MESH,
        )

    barrier = pltpu.get_barrier_semaphore()

    def greet_sp(o, _):
        pl.semaphore_signal(
            barrier, inc=1, device_id={"sp": lax.rem(sp + o, NSP)},
            device_id_type=pl.DeviceIdType.MESH,
        )
        return 0

    def greet_dp(o, _):
        pl.semaphore_signal(
            barrier, inc=1, device_id={"dp": lax.rem(dp + o, NDP)},
            device_id_type=pl.DeviceIdType.MESH,
        )
        return 0

    lax.fori_loop(1, NSP, greet_sp, 0)
    lax.fori_loop(1, NDP, greet_dp, 0)

    def cols(i, w):
        return pl.ds(pl.multiple_of(i * w, w), w)

    own = [
        pltpu.make_async_copy(q.at[:, cols(z, 512)], q_all.at[z], loc.at[0]),
        pltpu.make_async_copy(g.at[:, cols(z, 512)], g_all.at[z], loc.at[1]),
        pltpu.make_async_copy(v.at[:, cols(z, D)], v_all.at[x, z], loc.at[2]),
        pltpu.make_async_copy(li.at[:, cols(dp, 512)], li_all.at[dp], loc.at[3]),
        pltpu.make_async_copy(kw, kw_s, loc.at[4]),
        pltpu.make_async_copy(vw, vw_s, loc.at[5]),
    ]
    for c in own:
        c.start()

    for zz in range(NZ):
        shard = NX * zz + x
        for kind in range(3):
            part = tc[kind]
            tab[zz, kind, 0:64] = part + tr[kind, 2 * shard]
            tab[zz, kind, 64:128] = part + tr[kind, 2 * shard + 1]

    for h in range(NZ):
        u = k[:, h * D : (h + 1) * D].astype(F32)
        n = u * inv_rms(u) * kg[...]
        k_src[h] = rotate(n, tab[z, 0], tab[z, 1], tab[z, 2]).astype(BF)
    k_all[x, z] = k_src[z]

    with jax.named_scope("s_barrier"):
        pl.semaphore_wait(barrier, NSP + NDP - 2)

    def z_copies(o, side, kinds):
        peer = lax.rem(z + o, NZ)
        slot = z if side == "send" else peer
        pairs = (
            (k_src.at[peer], k_all.at[x, slot]),
            (v.at[:, cols(peer, D)], v_all.at[x, slot]),
            (q.at[:, cols(peer, 512)], q_all.at[slot]),
            (g.at[:, cols(peer, 512)], g_all.at[slot]),
        )
        return [
            remote(*pairs[i], zs.at[i, peer], zr.at[i, slot], sp=peer * NX + x) for i in kinds
        ]

    order = (1, 3, 2)
    own[2].wait()
    for o in order:
        for c in z_copies(o, "send", (0, 1)):
            c.start()

    kv = (k_all, v_all)

    def x_copy(kind, chunk, zz, peer):
        sem = rem4(peer - chunk)
        return remote(
            kv[kind].at[chunk, zz], kv[kind].at[chunk, zz], xs.at[kind, sem, zz],
            xr.at[kind, chunk, zz], sp=z * NX + peer,
        )

    def rem4(i):
        return lax.rem(i + 4, 4)

    def x_send(zz):
        for kind in range(2):
            x_copy(kind, x, zz, rem4(x + 1)).start()
            x_copy(kind, x, zz, rem4(x - 1)).start()

    x_send(z)
    for o in order:
        for c in z_copies(o, "send", (2, 3)):
            c.start()

    def li_copy(o, side):
        peer = lax.rem(dp + o, NDP)
        slot = dp if side == "send" else peer
        return remote(li.at[:, cols(peer, 512)], li_all.at[slot], lis.at[peer], lir.at[slot], dp=peer)

    def li_start(o, _):
        li_copy(o, "send").start()
        return 0

    lax.fori_loop(1, NDP, li_start, 0)

    def dq_copy(zz):
        return remote(dq_out.at[zz], gq.at[:, cols(z, 512)], dqs.at[zz], dqr.at[z], sp=zz * NX + x)

    def prepare(o):
        zz = lax.rem(z + o, NZ)
        for h in range(4):
            rows = pl.ds(pl.multiple_of(o * 512 + h * T, T), T)
            u = q_all[zz, :, h * D : (h + 1) * D].astype(F32)
            n = u * inv_rms(u) * qg[...]
            qs[rows, :] = rotate(n, tab[zz, 0], tab[zz, 1], tab[zz, 2]).astype(BF)
            gs[rows, :] = g_all[zz, :, h * D : (h + 1) * D]

    def unit(xo, o):
        xx = lax.rem(x + xo, NX)
        qcols = pl.ds(pl.multiple_of(o * 512, 512), 512)
        qb, gb = qs[qcols, :], gs[qcols, :]
        for half in range(2):
            kc = k_all[xx, 2 * half : 2 * half + 2].reshape(256, D)
            vc = v_all[xx, 2 * half : 2 * half + 2].reshape(256, D)
            rows = pl.ds(pl.multiple_of(xx * 512 + half * 256, 256), 256)
            s = dot_nt(kc, qb)
            s_all[rows, qcols] = s
            m_scr[:, qcols] = jnp.maximum(m_scr[:, qcols], jnp.max(s.reshape(32, 8, 512), axis=0))
            dp_all[rows, qcols] = dot_nt(vc, gb)

    def x_wait(kind, o, zz):
        chunk = rem4(x + o)
        x_copy(kind, chunk, zz, chunk).wait_recv()

    def wait_q(o):
        for c in z_copies(o, "recv", (2, 3)):
            c.wait_recv()

    def three(i):
        return i + i // 2

    m_scr[...] = jnp.full((8, 2048), -jnp.inf, F32)
    own[0].wait()
    own[1].wait()
    prepare(0)
    with jax.named_scope("s_zkv"):
        for o in order:
            for c in z_copies(o, "recv", (0, 1)):
                c.wait_recv()
            x_send(rem4(z + o))
    with jax.named_scope("s_u0"):
        unit(0, 0)
    with jax.named_scope("s_u1"):
        for o in (0, 1, 3, 2):
            zz = rem4(z + o)
            x_wait(0, 1, zz)
            x_copy(0, rem4(x + 1), zz, rem4(x - 1)).start()
            x_wait(1, 3, zz)
            x_copy(1, rem4(x - 1), zz, rem4(x + 1)).start()
            x_wait(0, 3, zz)
            x_wait(1, 1, zz)
        unit(1, 0)
        unit(3, 0)

    def near_queries(i, _):
        o = 1 + 2 * i
        wait_q(o)
        prepare(o)
        lax.fori_loop(0, 3, lambda j, _: (unit(three(j), o), 0)[1], 0)
        return 0

    with jax.named_scope("s_u2"):
        lax.fori_loop(0, 2, near_queries, 0)
    with jax.named_scope("s_u3"):
        for o in (0, 1, 3, 2):
            for kind in range(2):
                x_wait(kind, 2, rem4(z + o))
        lax.fori_loop(0, 3, lambda j, _: (unit(2, three(j)), 0)[1], 0)
    with jax.named_scope("s_u4"):
        wait_q(2)
        prepare(2)
        lax.fori_loop(0, 4, lambda j, _: (unit(j, 2), 0)[1], 0)
        k_t[...] = k_all[...].reshape(NSP * T, D).T

    def block_cols(i):
        return pl.ds(pl.multiple_of(i * 256, 256), 256)

    def soft(i, _):
        here = block_cols(i)
        m = jnp.max(m_scr[:, here], axis=0, keepdims=True) * EXP2_SCALE
        l8 = jnp.zeros((8, 256), F32)
        for j in range(2048 // KC):
            e = jnp.exp2(s_all[j * KC : (j + 1) * KC, here] * EXP2_SCALE - m)
            s_all[j * KC : (j + 1) * KC, here] = e
            l8 = l8 + jnp.sum(e.reshape(KC // 8, 8, 256), axis=0)
        rl = 1.0 / jnp.sum(l8, axis=0, keepdims=True)
        rl_scr[:, here] = jnp.broadcast_to(rl, (8, 256))
        d8 = jnp.zeros((8, 256), F32)
        for j in range(2048 // KC):
            at = slice(j * KC, (j + 1) * KC)
            p_b = (s_all[at, here] * rl).astype(BF)
            pb[at, here] = p_b
            prod = p_b.astype(F32) * dp_all[at, here]
            d8 = d8 + jnp.sum(prod.reshape(KC // 8, 8, 256), axis=0)
        d_scr[:, here] = d8
        return 0

    with jax.named_scope("s_soft"):
        lax.fori_loop(0, 8, soft, 0)

    def grads_out(left, right, src, into, which):
        def step(t, _):
            xx = lax.rem(x + 1 + t // 2, NX)
            half = lax.rem(t, 2)
            at = pl.ds(pl.multiple_of(xx * 512 + half * 256, 256), 256)
            out = dot_nn(left[at, :], right[...])
            src[xx, pl.ds(2 * half, 2)] = out.astype(BF).reshape(2, T, D)
            for j in range(2):
                zz = 2 * half + j
                peer = zz * NX + xx

                @pl.when(peer != sp)
                def _():
                    remote(
                        src.at[xx, zz], into.at[sp], dps.at[which, peer], dpr.at[which, sp], sp=peer
                    ).start()

            return 0

        lax.fori_loop(0, 2 * NX, step, 0)
        into[sp] = src[x, z]

    def wait_grads(src, into, which):
        def one(o, _):
            peer = lax.rem(sp + o, NSP)
            remote(src.at[0, 0], into.at[peer], dps.at[which, peer], dpr.at[which, peer], sp=peer).wait_recv()
            return 0

        lax.fori_loop(1, NSP, one, 0)

    def head_sum(into, h):
        total = into[NX * h].astype(F32)
        for xx in range(1, NX):
            total = total + into[NX * h + xx].astype(F32)
        return total

    def same(o, side, buf, which):
        peer = lax.rem(y + o, NY)
        slot = dp if side == "send" else 2 * peer + core
        return remote(buf.at[slot], buf.at[slot], as_.at[which, 2 * peer + core], ar.at[which, slot], dp=2 * peer + core)

    def cross(yy, side, buf, which):
        slot = 2 * yy + (core if side == "send" else 1 - core)
        return remote(buf.at[slot], buf.at[slot], as_.at[which + 2, yy], ar.at[which, slot], dp=2 * y + (1 - core))

    def gather_start(buf, which):
        for o in order:
            same(o, "send", buf, which).start()
        cross(y, "send", buf, which).start()

    def gather_finish(buf, which):
        for o in order:
            same(o, "recv", buf, which).wait_recv()
            cross(lax.rem(y + o, NY), "send", buf, which).start()
        for yy in range(NY):
            cross(yy, "recv", buf, which).wait_recv()

    def gi_src(peer):
        return pb.at[pl.ds(pl.multiple_of(peer * T, T), T), 512:1024]

    outs = (gwv, gwk)

    def stage_copy(stage, which, half, o, side):
        along_x = (half == 0) == (stage in (0, 3))
        me = x if along_x else z
        peer = rem4(me + o)
        slot = me if side == "send" else peer
        wide = slice(half * 256, (half + 1) * 256)

        def rows(i, n, base=0):
            return pl.ds(pl.multiple_of(base + i * n, n), n)

        if stage == 0:
            src, dst = pb.at[rows(peer, T, which * 512), wide], r1.at[which, half, slot]
        elif stage == 1:
            src, dst = st1.at[which, half, rows(peer, 32)], r2.at[which, half, slot]
        elif stage == 2:
            src = dst = go.at[which, half, rows(slot, 32)]
        else:
            src, dst = go.at[which, half], outs[which].at[rows(slot, T), wide]
        target = z * NX + peer if along_x else peer * NX + x
        return remote(
            src, dst, ts.at[stage, which, half, peer], tr_.at[stage, which, half, slot], sp=target
        )

    def stage_start(stage, which, half):
        for o in order:
            stage_copy(stage, which, half, o, "send").start()

    def stage_wait(stage, which, half):
        for o in order:
            stage_copy(stage, which, half, o, "recv").wait_recv()

    def own_part(which, half):
        group = x if half == 0 else z
        return pltpu.make_async_copy(
            go.at[which, half],
            outs[which].at[cols(group, T), half * 256 : (half + 1) * 256],
            loc.at[7 + 2 * which + half],
        )

    def reduce_start(buf, which):
        out = dot_tn(li_all[...].reshape(NDP * T, 512), buf[...].reshape(NDP * T, 512))
        pb[which * 512 : (which + 1) * 512, 0:512] = out.astype(BF)
        for half in range(2):
            stage_start(0, which, half)

    def reduce_first(which):
        for half in range(2):
            me = x if half == 0 else z
            stage_wait(0, which, half)
            at = pl.ds(pl.multiple_of(which * 512 + me * T, T), T)
            total = pb[at, half * 256 : (half + 1) * 256].astype(F32)
            for o in order:
                total = total + r1[which, half, rem4(me + o)].astype(F32)
            st1[which, half] = total.astype(BF)
            stage_start(1, which, half)

    def reduce_second(which):
        for half in range(2):
            me = z if half == 0 else x
            stage_wait(1, which, half)
            at = pl.ds(pl.multiple_of(me * 32, 32), 32)
            total = st1[which, half, at].astype(F32)
            for o in order:
                total = total + r2[which, half, rem4(me + o)].astype(F32)
            go[which, half, at] = total.astype(BF)
            stage_start(2, which, half)

    def spread(which):
        for half in range(2):
            stage_wait(2, which, half)
            stage_start(3, which, half)
            own_part(which, half).start()

    def scores(t, _):
        here = block_cols(t)
        delta = jnp.sum(d_scr[:, here], axis=0, keepdims=True)
        rl = rl_scr[0:1, here]
        for j in range(2048 // KC):
            at = slice(j * KC, (j + 1) * KC)
            ds[at, here] = ((s_all[at, here] * rl) * (dp_all[at, here] - delta)).astype(BF)
        return 0

    with jax.named_scope("s_scores"):
        lax.fori_loop(0, 8, scores, 0)
    with jax.named_scope("s_dk"):
        grads_out(ds, qs, dk_src, dk_in, 1)
    with jax.named_scope("s_dv"):
        grads_out(pb, gs, dv_src, dv_in, 0)

    def query_grads(i):
        off = i // 2
        zz = lax.rem(z + off, NZ)
        pair = lax.rem(i, 2)
        wide = pl.ds(pl.multiple_of(pair * 256, 256), 256)
        grad = dot_nn(k_t[...], ds[:, block_cols(i)]).T * SCALE
        both = q_all[zz, :, wide].astype(F32)
        outs = []
        for h in range(2):
            outs.append(
                norm_back(
                    grad[h * D : (h + 1) * D], both[:, h * D : (h + 1) * D], qg[...],
                    tab[zz, 0], tab[zz, 1], tab[zz, 2],
                ).astype(BF)
            )
        dq_out[zz, :, wide] = jnp.concatenate(outs, axis=1)

    def query_send(i):
        off = i // 2
        zz = lax.rem(z + off, NZ)
        pair = lax.rem(i, 2)

        @pl.when(i == 1)
        def _():
            pltpu.make_async_copy(dq_out.at[z], gq.at[:, cols(z, 512)], loc.at[6]).start()

        @pl.when((pair == 1) & (off > 0))
        def _():
            dq_copy(zz).start()

    def back(t, _):
        query_grads(t)
        query_send(t)
        return 0

    with jax.named_scope("s_dq1"):
        lax.fori_loop(0, 4, back, 0)
    with jax.named_scope("s_wdk"):
        wait_grads(dk_src, dk_in, 1)
    pieces = []
    for h in range(NZ):
        u = k[:, h * D : (h + 1) * D].astype(F32)
        pieces.append(
            norm_back(head_sum(dk_in, h) * SCALE, u, kg[...], tab[z, 0], tab[z, 1], tab[z, 2]).astype(BF)
        )
    ks_all[dp] = jnp.concatenate(pieces, axis=1)
    gather_start(ks_all, 1)

    with jax.named_scope("s_dq2"):
        lax.fori_loop(4, 8, back, 0)
    with jax.named_scope("s_wdv"):
        wait_grads(dv_src, dv_in, 0)
    vs_all[dp] = jnp.concatenate([head_sum(dv_in, h).astype(BF) for h in range(NZ)], axis=1)
    gather_start(vs_all, 0)
    own[3].wait()

    def li_wait(o, _):
        li_copy(o, "recv").wait_recv()
        return 0

    lax.fori_loop(1, NDP, li_wait, 0)

    with jax.named_scope("s_gfk"):
        gather_finish(ks_all, 1)
    with jax.named_scope("s_rsk"):
        reduce_start(ks_all, 1)
    with jax.named_scope("s_gfv"):
        gather_finish(vs_all, 0)
    with jax.named_scope("s_rsv"):
        reduce_start(vs_all, 0)

    own[4].wait()
    own[5].wait()

    def gi_copy(peer):
        return remote(gi_src(peer), gin.at[:, cols(dp, 512)], gis.at[peer], gir.at[dp], dp=peer)

    def grad_in(i, _):
        group = lax.rem(dp // 4 + 1 + i, 2)
        four = pl.ds(4 * group, 4)
        out = dot_nt(ks_all[four].reshape(512, 512), kw_s[...])
        out = out + dot_nt(vs_all[four].reshape(512, 512), vw_s[...])
        pb[pl.ds(pl.multiple_of(group * 512, 512), 512), 512:1024] = out.astype(BF)
        for j in range(4):
            peer = 4 * group + j

            @pl.when(peer != dp)
            def _():
                gi_copy(peer).start()

        return 0

    with jax.named_scope("s_gin"):
        lax.fori_loop(0, 2, grad_in, 0)
    pltpu.make_async_copy(gi_src(dp), gin.at[:, cols(dp, 512)], loc.at[11]).start()

    with jax.named_scope("s_rf1"):
        reduce_first(1)
        reduce_first(0)
    with jax.named_scope("s_rf2"):
        reduce_second(1)
        reduce_second(0)
    with jax.named_scope("s_rf3"):
        spread(1)
        spread(0)

    pltpu.make_async_copy(dq_out.at[z], gq.at[:, cols(z, 512)], loc.at[6]).wait()
    pltpu.make_async_copy(gi_src(dp), gin.at[:, cols(dp, 512)], loc.at[11]).wait()
    for o in range(1, NZ):
        for c in z_copies(o, "send", (0, 1, 2, 3)):
            c.wait_send()
        zz = lax.rem(z + o, NZ)
        dq_copy(zz).wait_send()
        remote(dq_out.at[zz], gq.at[:, cols(zz, 512)], dqs.at[zz], dqr.at[zz], sp=zz * NX + x).wait_recv()
    for which, buf in ((0, vs_all), (1, ks_all)):
        for o in range(1, NY):
            same(o, "send", buf, which).wait_send()
        for yy in range(NY):
            cross(yy, "send", buf, which).wait_send()

    for zz in range(NZ):
        for kind in range(2):
            x_copy(kind, x, zz, rem4(x + 1)).wait_send()
            x_copy(kind, x, zz, rem4(x - 1)).wait_send()
        x_copy(0, rem4(x + 1), zz, rem4(x - 1)).wait_send()
        x_copy(1, rem4(x - 1), zz, rem4(x + 1)).wait_send()

    def drain_dp(o, _):
        peer = lax.rem(dp + o, NDP)
        li_copy(o, "send").wait_send()
        gi_copy(peer).wait_send()
        remote(gi_src(peer), gin.at[:, cols(peer, 512)], gis.at[peer], gir.at[peer], dp=peer).wait_recv()
        return 0

    with jax.named_scope("s_drdp"):
        lax.fori_loop(1, NDP, drain_dp, 0)

    def drain_sp(o, _):
        peer = lax.rem(sp + o, NSP)
        for which, src, into in ((0, dv_src, dv_in), (1, dk_src, dk_in)):
            remote(src.at[0, 0], into.at[peer], dps.at[which, peer], dpr.at[which, peer], sp=peer).wait_send()
        return 0

    lax.fori_loop(1, NSP, drain_sp, 0)
    with jax.named_scope("s_drsp"):
        for which in range(2):
            for half in range(2):
                stage_wait(3, which, half)
                own_part(which, half).wait()
                for stage in range(4):
                    for o in order:
                        stage_copy(stage, which, half, o, "send").wait_send()


def on_device(queries, keys, values, out_grad, layer_in, key_weight, value_weight, query_gain, key_gain):
    rows, cols = rope_tables()
    hbm = pl.BlockSpec(memory_space=pl.ANY)
    vmem = pl.BlockSpec(memory_space=pltpu.VMEM)
    dma = pltpu.SemaphoreType.DMA
    V = pltpu.VMEM
    gq, gin, gwv, gwk = pl.pallas_call(
        body,
        out_shape=(
            jax.ShapeDtypeStruct((T, 2048), BF),
            jax.ShapeDtypeStruct((T, 4096), BF),
            jax.ShapeDtypeStruct((512, 512), BF),
            jax.ShapeDtypeStruct((512, 512), BF),
        ),
        in_specs=[hbm, vmem, hbm, hbm, hbm, hbm, hbm, vmem, vmem, vmem, vmem],
        out_specs=(hbm, hbm, hbm, hbm),
        scratch_shapes=[
            V((NZ, T, 512), BF),
            V((NZ, T, 512), BF),
            V((NX, NZ, T, D), BF),
            V((NX, NZ, T, D), BF),
            V((NZ, T, D), BF),
            V((D, 2048), BF),
            V((NZ, 3, T, D), F32),
            V((2048, D), BF),
            V((2048, D), BF),
            V((8, 2048), F32),
            V((8, 2048), F32),
            V((8, 2048), F32),
            V((2048, 2048), F32),
            V((2048, 2048), F32),
            V((2048, 2048), BF),
            V((2048, 2048), BF),
            V((NZ, T, 512), BF),
            V((NX, NZ, T, D), BF),
            V((NX, NZ, T, D), BF),
            V((NSP, T, D), BF),
            V((NSP, T, D), BF),
            V((NDP, T, 512), BF),
            V((512, 512), BF),
            V((512, 512), BF),
            V((NDP, T, 512), BF),
            V((NDP, T, 512), BF),
            V((2, 2, 4, T, 256), BF),
            V((2, 2, T, 256), BF),
            V((2, 2, 4, 32, 256), BF),
            V((2, 2, T, 256), BF),
            dma((12,)),
            dma((4, NZ)),
            dma((4, NZ)),
            dma((2, NX, NZ)),
            dma((2, NX, NZ)),
            dma((NDP,)),
            dma((NDP,)),
            dma((NZ,)),
            dma((NZ,)),
            dma((2, NSP)),
            dma((2, NSP)),
            dma((4, NDP)),
            dma((2, NDP)),
            dma((4, 2, 2, 4)),
            dma((4, 2, 2, 4)),
            dma((NDP,)),
            dma((NDP,)),
        ],
        compiler_params=pltpu.CompilerParams(
            collective_id=0, has_side_effects=True, vmem_limit_bytes=67043328
        ),
        name="step",
    )(
        queries[0], keys[0], values[0], out_grad[0], layer_in[0], key_weight, value_weight,
        query_gain.reshape(1, D), key_gain.reshape(1, D), jnp.asarray(rows), jnp.asarray(cols),
    )
    return gq[None], gin[None], gwk.astype(F32), gwv.astype(F32)


def solution(mesh):
    in_specs = (
        P("dp", "sp", None),
        P("dp", "sp", None),
        P("dp", "sp", None),
        P("dp", "sp", None),
        P("dp", "sp", None),
        P("dp", None),
        P("dp", None),
        P(),
        P(),
    )
    out_specs = (P("dp", "sp", None), P("dp", "sp", None), P("dp", None), P("dp", None))
    return jax.shard_map(
        on_device, mesh=mesh, in_specs=in_specs, out_specs=out_specs, check_vma=False
    )
```

time: 102 us -> 92.5 us (0.907)
  Pallas kernels: 96.4 us -> 86.5 us
    pallas_call x1, Pallas kernels: 96.4 us -> 86.5 us  [on_device(): pl.pallas_call(body, out_shape=(jax.ShapeDtypeStruct((T, 2048), BF), jax....]
    unnamed x6 -> x8, local copies, waits for them, and re-layouts: 2.38 us -> 1.77 us
    convert_element_type x1 -> x2, other arithmetic: 2.86 us -> 3.3 us  [on_device(): return (gq[None], gin[None], gwk.astype(F32), gwv.astype(F32))]
where the time goes in v3:
time: 92.5 us; the launch traced here: 92.2 us
  Pallas kernels  86.5 us (94%)
  other arithmetic  3.3 us (4%)
  local copies, waits for them, and re-layouts  1.77 us (2%)
    pallas_call x1, Pallas kernels, on_device(): pl.pallas_call(body, out_shape=(jax.ShapeDtypeStruct((T, 2048), BF), jax....  86.5 us
    convert_element_type x2, other arithmetic, on_device(): return (gq[None], gin[None], gwk.astype(F32), gwv.astype(F32))  3.3 us

profile of v3, /device:TPU:1, one launch (start us, length us, event | category | flops | bytes accessed | tf_op | source)
XLA Modules:
  0.0 92.2 jit_solution(3229034580454054920)
XLA Ops:
  0.6 86.5 %step.1 = (bf16[128,2048]{1,0:T(8,128)(2,1)}, bf16[128,4096]{1,0:T(8,128)(2,1)}, bf16[512,512]{1,0:T(8,128)(2,1)}, bf16[512,512]{1,0:T(8,128)(2,1)}) custom-call(bf16[128,2048]{1,0:T(8,128)(2,1)} %bitcast.12, bf16[128,512]{1,0:T(8,128)(2,1)} %bitcast.14, bf16[128,512]{1,0:T(8,128)(2,1)} %bitcast.15, bf16[128,2048]{1,0:T(8,128)(2,1)} %bitcast.13, ...), custom_call_target="tpu_custom_call" | custom-call | tf_op jit(solution)/shard_map/step/pallas_call | solution.py:615
  87.2 0.0 copy-start.1
  87.2 2.2 %convert_element_type.6 = f32[512,512]{1,0:T(8,128)} convert(bf16[512,512]{1,0:T(8,128)(2,1)} %get-tuple-element.10) | non-fusion elementwise | flops 262144 | bytes 1572864 | tf_op jit(solution)/shard_map/convert_element_type | solution.py:682
  89.4 0.0 copy-done.1
  89.4 0.0 copy-start.2
  89.4 0.0 copy-start
  89.4 1.1 %convert_element_type.7 = f32[512,512]{1,0:T(8,128)} convert(bf16[512,512]{1,0:T(8,128)(2,1)S(1)} %copy-done.1) | non-fusion elementwise | flops 262144 | bytes 1572864 | tf_op jit(solution)/shard_map/convert_element_type | solution.py:682
  90.5 0.0 copy-done.2
  90.5 0.8 copy.17
  91.3 0.0 copy-done
  91.3 1.0 %copy.18 = bf16[1,128,4096]{2,1,0:T(8,128)(2,1)} copy(bf16[1,128,4096]{2,1,0:T(8,128)(2,1)S(1)} %bitcast.9) | data formatting | bytes 2097152
Async XLA Ops:
  87.2 2.2 %copy-start.1 = (bf16[512,512]{1,0:T(8,128)(2,1)S(1)}, bf16[512,512]{1,0:T(8,128)(2,1)}, u32[]{:S(2)}) copy-start(bf16[512,512]{1,0:T(8,128)(2,1)} %get-tuple-element.11) | copy-start | bytes 1572868
  89.4 1.1 %copy-start.2 = (bf16[128,2048]{1,0:T(8,128)(2,1)S(1)}, bf16[128,2048]{1,0:T(8,128)(2,1)}, u32[]{:S(2)}) copy-start(bf16[128,2048]{1,0:T(8,128)(2,1)} %get-tuple-element.8) | copy-start | bytes 1572868
  89.4 1.9 %copy-start = (bf16[128,4096]{1,0:T(8,128)(2,1)S(1)}, bf16[128,4096]{1,0:T(8,128)(2,1)}, u32[]{:S(2)}) copy-start(bf16[128,4096]{1,0:T(8,128)(2,1)} %get-tuple-element.9) | copy-start | bytes 3145732

commit v4 on v3

--- a/solution.py
+++ b/solution.py
@@ -77,12 +77,12 @@
 
 
 def body(
-    q, k, v, g, li, kw, vw, qg, kg, tr, tc,
+    q, k_in, v, g, li, kw, vw, qg_in, kg_in, tr_in, tc_in,
     gq, gin, gwv, gwk,
-    q_all, g_all, k_all, v_all, k_src, k_t, tab, qs, gs, m_scr, rl_scr, d_scr, s_all, dp_all, pb, ds,
+    k, qg, kg, tr, tc, q_all, g_all, k_all, v_all, k_src, k_t, tab, qs, gs, m_scr, rl_scr, d_scr, s_all, dp_all, pb, ds,
     dq_out, dv_src, dk_src, dv_in, dk_in, li_all, kw_s, vw_s, vs_all, ks_all,
     r1, st1, r2, go,
-    loc, zs, zr, xs, xr, lis, lir, dqs, dqr, dps, dpr, as_, ar, ts, tr_, gis, gir,
+    loc, zs, zr, xs, xr, misc, dps, dpr, as_, ar, ts, trs,
 ):
     sp = lax.axis_index("sp")
     dp = lax.axis_index("dp")
@@ -95,6 +95,12 @@
             device_id=where, device_id_type=pl.DeviceIdType.MESH,
         )
 
+    def sent(ref, sem):
+        remote(ref, ref, sem, sem, sp=sp).wait_send()
+
+    def landed(ref, sem):
+        remote(ref, ref, sem, sem, sp=sp).wait_recv()
+
     barrier = pltpu.get_barrier_semaphore()
 
     def greet_sp(o, _):
@@ -117,6 +123,14 @@
     def cols(i, w):
         return pl.ds(pl.multiple_of(i * w, w), w)
 
+    small = [
+        pltpu.make_async_copy(src, dst, loc.at[7 + i])
+        for i, (src, dst) in enumerate(
+            ((k_in, k), (qg_in, qg), (kg_in, kg), (tr_in, tr), (tc_in, tc))
+        )
+    ]
+    for c in small:
+        c.start()
     own = [
         pltpu.make_async_copy(q.at[:, cols(z, 512)], q_all.at[z], loc.at[0]),
         pltpu.make_async_copy(g.at[:, cols(z, 512)], g_all.at[z], loc.at[1]),
@@ -127,6 +141,8 @@
     ]
     for c in own:
         c.start()
+    for c in small:
+        c.wait()
 
     for zz in range(NZ):
         shard = NX * zz + x
@@ -154,7 +170,7 @@
             (g.at[:, cols(peer, 512)], g_all.at[slot]),
         )
         return [
-            remote(*pairs[i], zs.at[i, peer], zr.at[i, slot], sp=peer * NX + x) for i in kinds
+            remote(*pairs[i], zs.at[i], zr.at[i // 2, slot], sp=peer * NX + x) for i in kinds
         ]
 
     order = (1, 3, 2)
@@ -165,30 +181,28 @@
 
     kv = (k_all, v_all)
 
-    def x_copy(kind, chunk, zz, peer):
-        sem = rem4(peer - chunk)
-        return remote(
-            kv[kind].at[chunk, zz], kv[kind].at[chunk, zz], xs.at[kind, sem, zz],
-            xr.at[kind, chunk, zz], sp=z * NX + peer,
-        )
-
     def rem4(i):
         return lax.rem(i + 4, 4)
 
+    def x_copy(kind, chunk, zz, peer, ss, rs):
+        at = kv[kind].at[chunk, zz]
+        return remote(at, at, xs.at[ss], xr.at[rs], sp=z * NX + peer)
+
     def x_send(zz):
-        for kind in range(2):
-            x_copy(kind, x, zz, rem4(x + 1)).start()
-            x_copy(kind, x, zz, rem4(x - 1)).start()
+        x_copy(0, x, zz, rem4(x - 1), 0, zz).start()
+        x_copy(1, x, zz, rem4(x + 1), 0, 4 + zz).start()
+        x_copy(0, x, zz, rem4(x + 1), 0, 8).start()
+        x_copy(1, x, zz, rem4(x - 1), 0, 8).start()
 
     x_send(z)
-    for o in order:
+    for o in (1, 3):
         for c in z_copies(o, "send", (2, 3)):
             c.start()
 
     def li_copy(o, side):
         peer = lax.rem(dp + o, NDP)
         slot = dp if side == "send" else peer
-        return remote(li.at[:, cols(peer, 512)], li_all.at[slot], lis.at[peer], lir.at[slot], dp=peer)
+        return remote(li.at[:, cols(peer, 512)], li_all.at[slot], misc.at[0], misc.at[1], dp=peer)
 
     def li_start(o, _):
         li_copy(o, "send").start()
@@ -197,7 +211,7 @@
     lax.fori_loop(1, NDP, li_start, 0)
 
     def dq_copy(zz):
-        return remote(dq_out.at[zz], gq.at[:, cols(z, 512)], dqs.at[zz], dqr.at[z], sp=zz * NX + x)
+        return remote(dq_out.at[zz], gq.at[:, cols(z, 512)], misc.at[2], misc.at[3], sp=zz * NX + x)
 
     def prepare(o):
         zz = lax.rem(z + o, NZ)
@@ -221,64 +235,13 @@
             m_scr[:, qcols] = jnp.maximum(m_scr[:, qcols], jnp.max(s.reshape(32, 8, 512), axis=0))
             dp_all[rows, qcols] = dot_nt(vc, gb)
 
-    def x_wait(kind, o, zz):
-        chunk = rem4(x + o)
-        x_copy(kind, chunk, zz, chunk).wait_recv()
-
-    def wait_q(o):
-        for c in z_copies(o, "recv", (2, 3)):
-            c.wait_recv()
-
-    def three(i):
-        return i + i // 2
-
     m_scr[...] = jnp.full((8, 2048), -jnp.inf, F32)
     own[0].wait()
     own[1].wait()
-    prepare(0)
-    with jax.named_scope("s_zkv"):
-        for o in order:
-            for c in z_copies(o, "recv", (0, 1)):
-                c.wait_recv()
-            x_send(rem4(z + o))
-    with jax.named_scope("s_u0"):
-        unit(0, 0)
-    with jax.named_scope("s_u1"):
-        for o in (0, 1, 3, 2):
-            zz = rem4(z + o)
-            x_wait(0, 1, zz)
-            x_copy(0, rem4(x + 1), zz, rem4(x - 1)).start()
-            x_wait(1, 3, zz)
-            x_copy(1, rem4(x - 1), zz, rem4(x + 1)).start()
-            x_wait(0, 3, zz)
-            x_wait(1, 1, zz)
-        unit(1, 0)
-        unit(3, 0)
-
-    def near_queries(i, _):
-        o = 1 + 2 * i
-        wait_q(o)
-        prepare(o)
-        lax.fori_loop(0, 3, lambda j, _: (unit(three(j), o), 0)[1], 0)
-        return 0
-
-    with jax.named_scope("s_u2"):
-        lax.fori_loop(0, 2, near_queries, 0)
-    with jax.named_scope("s_u3"):
-        for o in (0, 1, 3, 2):
-            for kind in range(2):
-                x_wait(kind, 2, rem4(z + o))
-        lax.fori_loop(0, 3, lambda j, _: (unit(2, three(j)), 0)[1], 0)
-    with jax.named_scope("s_u4"):
-        wait_q(2)
-        prepare(2)
-        lax.fori_loop(0, 4, lambda j, _: (unit(j, 2), 0)[1], 0)
-        k_t[...] = k_all[...].reshape(NSP * T, D).T
-
     def block_cols(i):
         return pl.ds(pl.multiple_of(i * 256, 256), 256)
 
-    def soft(i, _):
+    def soft(i):
         here = block_cols(i)
         m = jnp.max(m_scr[:, here], axis=0, keepdims=True) * EXP2_SCALE
         l8 = jnp.zeros((8, 256), F32)
@@ -296,11 +259,57 @@
             prod = p_b.astype(F32) * dp_all[at, here]
             d8 = d8 + jnp.sum(prod.reshape(KC // 8, 8, 256), axis=0)
         d_scr[:, here] = d8
+
+    def scores(t):
+        here = block_cols(t)
+        delta = jnp.sum(d_scr[:, here], axis=0, keepdims=True)
+        rl = rl_scr[0:1, here]
+        for j in range(2048 // KC):
+            at = slice(j * KC, (j + 1) * KC)
+            ds[at, here] = ((s_all[at, here] * rl) * (dp_all[at, here] - delta)).astype(BF)
+
+    prepare(0)
+    with jax.named_scope("s_zkv"):
+        for o in order:
+            landed(k_src.at[0:2], zr.at[0, rem4(z + o)])
+            x_send(rem4(z + o))
+        for c in z_copies(2, "send", (2, 3)):
+            c.start()
+    with jax.named_scope("s_u0"):
+        unit(0, 0)
+    with jax.named_scope("s_u1"):
+        for o in (0, 1, 3, 2):
+            zz = rem4(z + o)
+            landed(k_src.at[0], xr.at[zz])
+            x_copy(0, rem4(x + 1), zz, rem4(x - 1), 1, 9).start()
+            landed(k_src.at[0], xr.at[4 + zz])
+            x_copy(1, rem4(x - 1), zz, rem4(x + 1), 1, 9).start()
+        landed(k_all.at[0:2], xr.at[8])
+        unit(1, 0)
+        unit(3, 0)
+        landed(k_all.at[0:2], xr.at[9])
+        unit(2, 0)
+
+    def block(i, _):
+        soft(i)
+        scores(i)
         return 0
 
-    with jax.named_scope("s_soft"):
-        lax.fori_loop(0, 8, soft, 0)
-
+    with jax.named_scope("s_b0"):
+        lax.fori_loop(0, 2, block, 0)
+
+    def shard(i, _):
+        o = 1 + 2 * i - 3 * (i // 2)
+        with jax.named_scope("s_qw"):
+            landed(q_all.at[0:2], zr.at[1, rem4(z + o)])
+        prepare(o)
+        lax.fori_loop(0, 4, lambda j, _: (unit(j, o), 0)[1], 0)
+        lax.fori_loop(2 * o, 2 * o + 2, block, 0)
+        return 0
+
+    with jax.named_scope("s_b1"):
+        lax.fori_loop(0, 3, shard, 0)
+    k_t[...] = k_all[...].reshape(NSP * T, D).T
     def grads_out(left, right, src, into, which):
         def step(t, _):
             xx = lax.rem(x + 1 + t // 2, NX)
@@ -315,7 +324,7 @@
                 @pl.when(peer != sp)
                 def _():
                     remote(
-                        src.at[xx, zz], into.at[sp], dps.at[which, peer], dpr.at[which, sp], sp=peer
+                        src.at[xx, zz], into.at[sp], dps.at[which], dpr.at[which], sp=peer
                     ).start()
 
             return 0
@@ -323,13 +332,8 @@
         lax.fori_loop(0, 2 * NX, step, 0)
         into[sp] = src[x, z]
 
-    def wait_grads(src, into, which):
-        def one(o, _):
-            peer = lax.rem(sp + o, NSP)
-            remote(src.at[0, 0], into.at[peer], dps.at[which, peer], dpr.at[which, peer], sp=peer).wait_recv()
-            return 0
-
-        lax.fori_loop(1, NSP, one, 0)
+    def wait_grads(into, which):
+        landed(into.at[0 : NSP - 1], dpr.at[which])
 
     def head_sum(into, h):
         total = into[NX * h].astype(F32)
@@ -337,69 +341,62 @@
             total = total + into[NX * h + xx].astype(F32)
         return total
 
-    def same(o, side, buf, which):
-        peer = lax.rem(y + o, NY)
-        slot = dp if side == "send" else 2 * peer + core
-        return remote(buf.at[slot], buf.at[slot], as_.at[which, 2 * peer + core], ar.at[which, slot], dp=2 * peer + core)
-
-    def cross(yy, side, buf, which):
-        slot = 2 * yy + (core if side == "send" else 1 - core)
-        return remote(buf.at[slot], buf.at[slot], as_.at[which + 2, yy], ar.at[which, slot], dp=2 * y + (1 - core))
+    def same(o, buf, which):
+        peer = rem4(y + o)
+        return remote(
+            buf.at[dp], buf.at[dp], as_.at[which], ar.at[which, y], dp=2 * peer + core
+        )
+
+    def cross(yy, buf, which):
+        slot = 2 * yy + core
+        return remote(
+            buf.at[slot], buf.at[slot], as_.at[which], ar.at[which, 4], dp=2 * y + (1 - core)
+        )
 
     def gather_start(buf, which):
         for o in order:
-            same(o, "send", buf, which).start()
-        cross(y, "send", buf, which).start()
+            same(o, buf, which).start()
+        cross(y, buf, which).start()
 
     def gather_finish(buf, which):
         for o in order:
-            same(o, "recv", buf, which).wait_recv()
-            cross(lax.rem(y + o, NY), "send", buf, which).start()
-        for yy in range(NY):
-            cross(yy, "recv", buf, which).wait_recv()
+            yy = rem4(y + o)
+            landed(buf.at[0], ar.at[which, yy])
+            cross(yy, buf, which).start()
+        landed(buf.at[0:4], ar.at[which, 4])
 
     def gi_src(peer):
         return pb.at[pl.ds(pl.multiple_of(peer * T, T), T), 512:1024]
 
     outs = (gwv, gwk)
 
-    def stage_copy(stage, which, half, o, side):
-        along_x = (half == 0) == (stage in (0, 3))
+    def stage_copy(stage, which, half, o):
+        along_x = (half == 0) == (stage != 1)
         me = x if along_x else z
         peer = rem4(me + o)
-        slot = me if side == "send" else peer
         wide = slice(half * 256, (half + 1) * 256)
-
-        def rows(i, n, base=0):
-            return pl.ds(pl.multiple_of(base + i * n, n), n)
-
         if stage == 0:
-            src, dst = pb.at[rows(peer, T, which * 512), wide], r1.at[which, half, slot]
+            src = pb.at[pl.ds(pl.multiple_of(which * 512 + peer * T, T), T), wide]
+            dst = r1.at[which, half, me]
         elif stage == 1:
-            src, dst = st1.at[which, half, rows(peer, 32)], r2.at[which, half, slot]
-        elif stage == 2:
-            src = dst = go.at[which, half, rows(slot, 32)]
+            src, dst = st1.at[which, half], r2.at[which, half, me]
         else:
-            src, dst = go.at[which, half], outs[which].at[rows(slot, T), wide]
+            src, dst = go.at[which, half], outs[which].at[cols(me, T), wide]
         target = z * NX + peer if along_x else peer * NX + x
-        return remote(
-            src, dst, ts.at[stage, which, half, peer], tr_.at[stage, which, half, slot], sp=target
-        )
+        return remote(src, dst, ts.at[stage], trs.at[stage, which, half], sp=target)
 
     def stage_start(stage, which, half):
         for o in order:
-            stage_copy(stage, which, half, o, "send").start()
+            stage_copy(stage, which, half, o).start()
 
     def stage_wait(stage, which, half):
-        for o in order:
-            stage_copy(stage, which, half, o, "recv").wait_recv()
+        landed(r1.at[which, half, 0:3], trs.at[stage, which, half])
 
     def own_part(which, half):
-        group = x if half == 0 else z
         return pltpu.make_async_copy(
             go.at[which, half],
-            outs[which].at[cols(group, T), half * 256 : (half + 1) * 256],
-            loc.at[7 + 2 * which + half],
+            outs[which].at[cols(x if half == 0 else z, T), half * 256 : (half + 1) * 256],
+            loc.at[12 + 2 * which + half],
         )
 
     def reduce_start(buf, which):
@@ -423,30 +420,13 @@
         for half in range(2):
             me = z if half == 0 else x
             stage_wait(1, which, half)
-            at = pl.ds(pl.multiple_of(me * 32, 32), 32)
-            total = st1[which, half, at].astype(F32)
+            total = st1[which, half].astype(F32)
             for o in order:
                 total = total + r2[which, half, rem4(me + o)].astype(F32)
-            go[which, half, at] = total.astype(BF)
+            go[which, half] = total.astype(BF)
             stage_start(2, which, half)
-
-    def spread(which):
-        for half in range(2):
-            stage_wait(2, which, half)
-            stage_start(3, which, half)
             own_part(which, half).start()
 
-    def scores(t, _):
-        here = block_cols(t)
-        delta = jnp.sum(d_scr[:, here], axis=0, keepdims=True)
-        rl = rl_scr[0:1, here]
-        for j in range(2048 // KC):
-            at = slice(j * KC, (j + 1) * KC)
-            ds[at, here] = ((s_all[at, here] * rl) * (dp_all[at, here] - delta)).astype(BF)
-        return 0
-
-    with jax.named_scope("s_scores"):
-        lax.fori_loop(0, 8, scores, 0)
     with jax.named_scope("s_dk"):
         grads_out(ds, qs, dk_src, dk_in, 1)
     with jax.named_scope("s_dv"):
@@ -490,7 +470,7 @@
     with jax.named_scope("s_dq1"):
         lax.fori_loop(0, 4, back, 0)
     with jax.named_scope("s_wdk"):
-        wait_grads(dk_src, dk_in, 1)
+        wait_grads(dk_in, 1)
     pieces = []
     for h in range(NZ):
         u = k[:, h * D : (h + 1) * D].astype(F32)
@@ -503,17 +483,12 @@
     with jax.named_scope("s_dq2"):
         lax.fori_loop(4, 8, back, 0)
     with jax.named_scope("s_wdv"):
-        wait_grads(dv_src, dv_in, 0)
+        wait_grads(dv_in, 0)
     vs_all[dp] = jnp.concatenate([head_sum(dv_in, h).astype(BF) for h in range(NZ)], axis=1)
     gather_start(vs_all, 0)
     own[3].wait()
 
-    def li_wait(o, _):
-        li_copy(o, "recv").wait_recv()
-        return 0
-
-    lax.fori_loop(1, NDP, li_wait, 0)
-
+    landed(li_all.at[0 : NDP - 1], misc.at[1])
     with jax.named_scope("s_gfk"):
         gather_finish(ks_all, 1)
     with jax.named_scope("s_rsk"):
@@ -527,7 +502,7 @@
     own[5].wait()
 
     def gi_copy(peer):
-        return remote(gi_src(peer), gin.at[:, cols(dp, 512)], gis.at[peer], gir.at[dp], dp=peer)
+        return remote(gi_src(peer), gin.at[:, cols(dp, 512)], misc.at[4], misc.at[5], dp=peer)
 
     def grad_in(i, _):
         group = lax.rem(dp // 4 + 1 + i, 2)
@@ -546,7 +521,7 @@
 
     with jax.named_scope("s_gin"):
         lax.fori_loop(0, 2, grad_in, 0)
-    pltpu.make_async_copy(gi_src(dp), gin.at[:, cols(dp, 512)], loc.at[11]).start()
+    pltpu.make_async_copy(gi_src(dp), gin.at[:, cols(dp, 512)], loc.at[16]).start()
 
     with jax.named_scope("s_rf1"):
         reduce_first(1)
@@ -554,62 +529,71 @@
     with jax.named_scope("s_rf2"):
         reduce_second(1)
         reduce_second(0)
-    with jax.named_scope("s_rf3"):
-        spread(1)
-        spread(0)
-
+    sent(k_src.at[0:3], zs.at[0])
+    sent(k_src.at[0:3], zs.at[1])
+    sent(q_all.at[0:3], zs.at[2])
+    sent(q_all.at[0:3], zs.at[3])
+    sent(k_all, xs.at[0])
+    sent(k_all.at[0:2], xs.at[1])
+    sent(li_all.at[0 : NDP - 1], misc.at[0])
+    sent(dq_out.at[0:3], misc.at[2])
+    landed(dq_out.at[0:3], misc.at[3])
+    for which, buf in ((0, vs_all), (1, ks_all)):
+        sent(dv_in.at[0 : NSP - 1], dps.at[which])
+        sent(buf.at[0 : NDP - 1], as_.at[which])
     pltpu.make_async_copy(dq_out.at[z], gq.at[:, cols(z, 512)], loc.at[6]).wait()
-    pltpu.make_async_copy(gi_src(dp), gin.at[:, cols(dp, 512)], loc.at[11]).wait()
-    for o in range(1, NZ):
-        for c in z_copies(o, "send", (0, 1, 2, 3)):
-            c.wait_send()
-        zz = lax.rem(z + o, NZ)
-        dq_copy(zz).wait_send()
-        remote(dq_out.at[zz], gq.at[:, cols(zz, 512)], dqs.at[zz], dqr.at[zz], sp=zz * NX + x).wait_recv()
-    for which, buf in ((0, vs_all), (1, ks_all)):
-        for o in range(1, NY):
-            same(o, "send", buf, which).wait_send()
-        for yy in range(NY):
-            cross(yy, "send", buf, which).wait_send()
-
-    for zz in range(NZ):
-        for kind in range(2):
-            x_copy(kind, x, zz, rem4(x + 1)).wait_send()
-            x_copy(kind, x, zz, rem4(x - 1)).wait_send()
-        x_copy(0, rem4(x + 1), zz, rem4(x - 1)).wait_send()
-        x_copy(1, rem4(x - 1), zz, rem4(x + 1)).wait_send()
-
-    def drain_dp(o, _):
-        peer = lax.rem(dp + o, NDP)
-        li_copy(o, "send").wait_send()
-        gi_copy(peer).wait_send()
-        remote(gi_src(peer), gin.at[:, cols(peer, 512)], gis.at[peer], gir.at[peer], dp=peer).wait_recv()
-        return 0
-
+    pltpu.make_async_copy(gi_src(dp), gin.at[:, cols(dp, 512)], loc.at[16]).wait()
     with jax.named_scope("s_drdp"):
-        lax.fori_loop(1, NDP, drain_dp, 0)
-
-    def drain_sp(o, _):
-        peer = lax.rem(sp + o, NSP)
-        for which, src, into in ((0, dv_src, dv_in), (1, dk_src, dk_in)):
-            remote(src.at[0, 0], into.at[peer], dps.at[which, peer], dpr.at[which, peer], sp=peer).wait_send()
-        return 0
-
-    lax.fori_loop(1, NSP, drain_sp, 0)
+        sent(li_all.at[0 : NDP - 1], misc.at[4])
+        landed(li_all.at[0 : NDP - 1], misc.at[5])
     with jax.named_scope("s_drsp"):
-        for which in range(2):
+        for which in (1, 0):
             for half in range(2):
-                stage_wait(3, which, half)
+                stage_wait(2, which, half)
                 own_part(which, half).wait()
-                for stage in range(4):
-                    for o in order:
-                        stage_copy(stage, which, half, o, "send").wait_send()
+        for stage in range(3):
+            sent(r1.at[:, :, 0:3], ts.at[stage])
+
+
+def finish(gq_in, gin_in, gwv_in, gwk_in, gq, gin, gwv, gwk, a, b, c, e, sem):
+    ins, outs = [], []
+    for i in range(4):
+        at = slice(i * 32, (i + 1) * 32)
+        rows = slice(i * T, (i + 1) * T)
+        ins.append(
+            [
+                pltpu.make_async_copy(gwk_in.at[rows], c.at[0, rows], sem.at[0, i, 0]),
+                pltpu.make_async_copy(gwv_in.at[rows], c.at[1, rows], sem.at[0, i, 1]),
+                pltpu.make_async_copy(gin_in.at[at], b.at[at], sem.at[0, i, 2]),
+                pltpu.make_async_copy(gq_in.at[at], a.at[at], sem.at[0, i, 3]),
+            ]
+        )
+        outs.append(
+            [
+                pltpu.make_async_copy(e.at[0, rows], gwk.at[rows], sem.at[1, i, 0]),
+                pltpu.make_async_copy(e.at[1, rows], gwv.at[rows], sem.at[1, i, 1]),
+                pltpu.make_async_copy(b.at[at], gin.at[at], sem.at[1, i, 2]),
+                pltpu.make_async_copy(a.at[at], gq.at[at], sem.at[1, i, 3]),
+            ]
+        )
+    for group in ins:
+        for copy in group:
+            copy.start()
+    for i in range(4):
+        rows = slice(i * T, (i + 1) * T)
+        for j in range(4):
+            ins[i][j].wait()
+            if j < 2:
+                e[j, rows] = c[j, rows].astype(F32)
+            outs[i][j].start()
+    for group in outs:
+        for copy in group:
+            copy.wait()
 
 
 def on_device(queries, keys, values, out_grad, layer_in, key_weight, value_weight, query_gain, key_gain):
     rows, cols = rope_tables()
     hbm = pl.BlockSpec(memory_space=pl.ANY)
-    vmem = pl.BlockSpec(memory_space=pltpu.VMEM)
     dma = pltpu.SemaphoreType.DMA
     V = pltpu.VMEM
     gq, gin, gwv, gwk = pl.pallas_call(
@@ -620,9 +604,14 @@
             jax.ShapeDtypeStruct((512, 512), BF),
             jax.ShapeDtypeStruct((512, 512), BF),
         ),
-        in_specs=[hbm, vmem, hbm, hbm, hbm, hbm, hbm, vmem, vmem, vmem, vmem],
+        in_specs=[hbm] * 11,
         out_specs=(hbm, hbm, hbm, hbm),
         scratch_shapes=[
+            V((T, 512), BF),
+            V((1, D), F32),
+            V((1, D), F32),
+            V(rows.shape, F32),
+            V(cols.shape, F32),
             V((NZ, T, 512), BF),
             V((NZ, T, 512), BF),
             V((NX, NZ, T, D), BF),
@@ -651,25 +640,20 @@
             V((NDP, T, 512), BF),
             V((2, 2, 4, T, 256), BF),
             V((2, 2, T, 256), BF),
-            V((2, 2, 4, 32, 256), BF),
+            V((2, 2, 4, T, 256), BF),
             V((2, 2, T, 256), BF),
-            dma((12,)),
-            dma((4, NZ)),
-            dma((4, NZ)),
-            dma((2, NX, NZ)),
-            dma((2, NX, NZ)),
-            dma((NDP,)),
-            dma((NDP,)),
-            dma((NZ,)),
-            dma((NZ,)),
-            dma((2, NSP)),
-            dma((2, NSP)),
-            dma((4, NDP)),
-            dma((2, NDP)),
-            dma((4, 2, 2, 4)),
-            dma((4, 2, 2, 4)),
-            dma((NDP,)),
-            dma((NDP,)),
+            dma((17,)),
+            dma((4,)),
+            dma((2, NZ)),
+            dma((2,)),
+            dma((10,)),
+            dma((6,)),
+            dma((2,)),
+            dma((2,)),
+            dma((2,)),
+            dma((2, 5)),
+            dma((3,)),
+            dma((3, 2, 2)),
         ],
         compiler_params=pltpu.CompilerParams(
             collective_id=0, has_side_effects=True, vmem_limit_bytes=67043328
@@ -679,7 +663,26 @@
         queries[0], keys[0], values[0], out_grad[0], layer_in[0], key_weight, value_weight,
         query_gain.reshape(1, D), key_gain.reshape(1, D), jnp.asarray(rows), jnp.asarray(cols),
     )
-    return gq[None], gin[None], gwk.astype(F32), gwv.astype(F32)
+    gq, gin, gwv, gwk = pl.pallas_call(
+        finish,
+        out_shape=(
+            jax.ShapeDtypeStruct((T, 2048), BF),
+            jax.ShapeDtypeStruct((T, 4096), BF),
+            jax.ShapeDtypeStruct((512, 512), F32),
+            jax.ShapeDtypeStruct((512, 512), F32),
+        ),
+        in_specs=[hbm] * 4,
+        out_specs=(hbm,) * 4,
+        scratch_shapes=[
+            V((T, 2048), BF),
+            V((T, 4096), BF),
+            V((2, 512, 512), BF),
+            V((2, 512, 512), F32),
+            dma((2, 4, 4)),
+        ],
+        name="finish",
+    )(gq, gin, gwv, gwk)
+    return gq[None], gin[None], gwk, gwv
 
 
 def solution(mesh):

time: 92.5 us -> 85.7 us (0.926)
  other arithmetic: 3.3 us -> 0 us
  local copies, waits for them, and re-layouts: 1.77 us -> 0 us
  Pallas kernels: 86.5 us -> 84.8 us
    pallas_call x1, Pallas kernels: 86.5 us -> 81.8 us  [on_device(): pl.pallas_call(body, out_shape=(jax.ShapeDtypeStruct((T, 2048), BF), jax....]
    convert_element_type x2 -> x0, other arithmetic: 3.3 us -> none  [on_device(): return (gq[None], gin[None], gwk.astype(F32), gwv.astype(F32))]
    pallas_call x0 -> x1, Pallas kernels: none -> 3.02 us  [on_device(): pl.pallas_call(finish, out_shape=(jax.ShapeDtypeStruct((T, 2048), BF), ja...]
    unnamed x8 -> x0, local copies, waits for them, and re-layouts: 1.77 us -> none
where the time goes in v4:
time: 85.7 us; the launch traced here: 85.5 us
  Pallas kernels  84.8 us (99%)
    pallas_call x1, Pallas kernels, on_device(): pl.pallas_call(body, out_shape=(jax.ShapeDtypeStruct((T, 2048), BF), jax....  81.8 us
    pallas_call x1, Pallas kernels, on_device(): pl.pallas_call(finish, out_shape=(jax.ShapeDtypeStruct((T, 2048), BF), ja...  3.02 us

profile of v4, /device:TPU:1, one launch (start us, length us, event | category | flops | bytes accessed | tf_op | source)
XLA Modules:
  0.0 85.5 jit_solution(9037137507224245484)
XLA Ops:
  0.6 81.8 %step.1 = (bf16[128,2048]{1,0:T(8,128)(2,1)}, bf16[128,4096]{1,0:T(8,128)(2,1)}, bf16[512,512]{1,0:T(8,128)(2,1)}, bf16[512,512]{1,0:T(8,128)(2,1)}) custom-call(bf16[128,2048]{1,0:T(8,128)(2,1)} %bitcast.10, bf16[128,512]{1,0:T(8,128)(2,1)} %bitcast.12, bf16[128,512]{1,0:T(8,128)(2,1)} %bitcast.13, bf16[128,2048]{1,0:T(8,128)(2,1)} %bitcast.11, ...), custom_call_target="tpu_custom_call" | custom-call | tf_op jit(solution)/shard_map/step/pallas_call | solution.py:599
  82.5 3.0 %finish.1 = (bf16[128,2048]{1,0:T(8,128)(2,1)}, bf16[128,4096]{1,0:T(8,128)(2,1)}, f32[512,512]{1,0:T(8,128)}, f32[512,512]{1,0:T(8,128)}) custom-call(bf16[128,2048]{1,0:T(8,128)(2,1)} %get-tuple-element.12.gq_in, bf16[128,4096]{1,0:T(8,128)(2,1)} %get-tuple-element.13.gin_in, bf16[512,512]{1,0:T(8,128)(2,1)} %get-tuple-element.14.gwv_in, ...), custom_call_target="tpu_custom_call" | custom-call | tf_op jit(solution)/shard_map/finish/pallas_call | solution.py:666

commit v5 on v4

--- a/solution.py
+++ b/solution.py
@@ -80,7 +80,7 @@
     q, k_in, v, g, li, kw, vw, qg_in, kg_in, tr_in, tc_in,
     gq, gin, gwv, gwk,
     k, qg, kg, tr, tc, q_all, g_all, k_all, v_all, k_src, k_t, tab, qs, gs, m_scr, rl_scr, d_scr, s_all, dp_all, pb, ds,
-    dq_out, dv_src, dk_src, dv_in, dk_in, li_all, kw_s, vw_s, vs_all, ks_all,
+    dq_out, dk_src, dv_in, dk_in, li_all, kw_s, vw_s, vs_all, ks_all,
     r1, st1, r2, go,
     loc, zs, zr, xs, xr, misc, dps, dpr, as_, ar, ts, trs,
 ):
@@ -231,9 +231,12 @@
             vc = v_all[xx, 2 * half : 2 * half + 2].reshape(256, D)
             rows = pl.ds(pl.multiple_of(xx * 512 + half * 256, 256), 256)
             s = dot_nt(kc, qb)
-            s_all[rows, qcols] = s
+            s_all[2 * o, rows, :] = s[:, :256]
+            s_all[2 * o + 1, rows, :] = s[:, 256:]
             m_scr[:, qcols] = jnp.maximum(m_scr[:, qcols], jnp.max(s.reshape(32, 8, 512), axis=0))
-            dp_all[rows, qcols] = dot_nt(vc, gb)
+            w = dot_nt(vc, gb)
+            dp_all[2 * o, rows, :] = w[:, :256]
+            dp_all[2 * o + 1, rows, :] = w[:, 256:]
 
     m_scr[...] = jnp.full((8, 2048), -jnp.inf, F32)
     own[0].wait()
@@ -241,32 +244,56 @@
     def block_cols(i):
         return pl.ds(pl.multiple_of(i * 256, 256), 256)
 
+    def exps(i, j, m, l8):
+        at = slice(j * KC, (j + 1) * KC)
+        e = jnp.exp2(s_all[i, at, :] * EXP2_SCALE - m)
+        s_all[i, at, :] = e
+        return l8 + jnp.sum(e.reshape(KC // 8, 8, 256), axis=0)
+
     def soft(i):
-        here = block_cols(i)
-        m = jnp.max(m_scr[:, here], axis=0, keepdims=True) * EXP2_SCALE
+        m = jnp.max(m_scr[:, block_cols(i)], axis=0, keepdims=True) * EXP2_SCALE
         l8 = jnp.zeros((8, 256), F32)
         for j in range(2048 // KC):
-            e = jnp.exp2(s_all[j * KC : (j + 1) * KC, here] * EXP2_SCALE - m)
-            s_all[j * KC : (j + 1) * KC, here] = e
-            l8 = l8 + jnp.sum(e.reshape(KC // 8, 8, 256), axis=0)
+            l8 = exps(i, j, m, l8)
+        probs(i, l8)
+
+    def whole(i):
+        rows = pl.ds(pl.multiple_of(i * 256, 256), 256)
+        qb, gb = qs[rows, :], gs[rows, :]
+        m8 = jnp.full((8, 256), -jnp.inf, F32)
+        for j in range(NX):
+            s = dot_nt(k_all[j].reshape(512, D), qb)
+            s_all[i, j * 512 : (j + 1) * 512, :] = s
+            m8 = jnp.maximum(m8, jnp.max(s.reshape(64, 8, 256), axis=0))
+        m = jnp.max(m8, axis=0, keepdims=True) * EXP2_SCALE
+        l8 = jnp.zeros((8, 256), F32)
+        for j in range(2 * NX):
+            vb = v_all[j // 2, 2 * (j % 2) : 2 * (j % 2) + 2].reshape(256, D)
+            dp_all[i, j * 256 : (j + 1) * 256, :] = dot_nt(vb, gb)
+            for n in range(4):
+                l8 = exps(i, 4 * j + n, m, l8)
+        probs(i, l8)
+
+    def probs(i, l8):
+        here = block_cols(i)
         rl = 1.0 / jnp.sum(l8, axis=0, keepdims=True)
         rl_scr[:, here] = jnp.broadcast_to(rl, (8, 256))
         d8 = jnp.zeros((8, 256), F32)
         for j in range(2048 // KC):
             at = slice(j * KC, (j + 1) * KC)
-            p_b = (s_all[at, here] * rl).astype(BF)
-            pb[at, here] = p_b
-            prod = p_b.astype(F32) * dp_all[at, here]
+            p_b = (s_all[i, at, :] * rl).astype(BF)
+            pb[i, at, :] = p_b
+            prod = p_b.astype(F32) * dp_all[i, at, :]
             d8 = d8 + jnp.sum(prod.reshape(KC // 8, 8, 256), axis=0)
         d_scr[:, here] = d8
 
-    def scores(t):
-        here = block_cols(t)
+    def scores(i):
+        here = block_cols(i)
         delta = jnp.sum(d_scr[:, here], axis=0, keepdims=True)
         rl = rl_scr[0:1, here]
         for j in range(2048 // KC):
             at = slice(j * KC, (j + 1) * KC)
-            ds[at, here] = ((s_all[at, here] * rl) * (dp_all[at, here] - delta)).astype(BF)
+            ds[i, at, :] = ((s_all[i, at, :] * rl) * (dp_all[i, at, :] - delta)).astype(BF)
 
     prepare(0)
     with jax.named_scope("s_zkv"):
@@ -298,13 +325,17 @@
     with jax.named_scope("s_b0"):
         lax.fori_loop(0, 2, block, 0)
 
+    def whole_block(i, _):
+        whole(i)
+        scores(i)
+        return 0
+
     def shard(i, _):
         o = 1 + 2 * i - 3 * (i // 2)
         with jax.named_scope("s_qw"):
             landed(q_all.at[0:2], zr.at[1, rem4(z + o)])
         prepare(o)
-        lax.fori_loop(0, 4, lambda j, _: (unit(j, o), 0)[1], 0)
-        lax.fori_loop(2 * o, 2 * o + 2, block, 0)
+        lax.fori_loop(2 * o, 2 * o + 2, whole_block, 0)
         return 0
 
     with jax.named_scope("s_b1"):
@@ -315,8 +346,11 @@
             xx = lax.rem(x + 1 + t // 2, NX)
             half = lax.rem(t, 2)
             at = pl.ds(pl.multiple_of(xx * 512 + half * 256, 256), 256)
-            out = dot_nn(left[at, :], right[...])
-            src[xx, pl.ds(2 * half, 2)] = out.astype(BF).reshape(2, T, D)
+            out = dot_nn(left[0, at, :], right[0:256, :])
+            for j in range(1, 8):
+                out = out + dot_nn(left[j, at, :], right[j * 256 : (j + 1) * 256, :])
+            for j in range(2):
+                src(xx, 2 * half + j)[...] = out[j * T : (j + 1) * T].astype(BF)
             for j in range(2):
                 zz = 2 * half + j
                 peer = zz * NX + xx
@@ -324,13 +358,13 @@
                 @pl.when(peer != sp)
                 def _():
                     remote(
-                        src.at[xx, zz], into.at[sp], dps.at[which], dpr.at[which], sp=peer
+                        src(xx, zz), into.at[sp], dps.at[which], dpr.at[which], sp=peer
                     ).start()
 
             return 0
 
         lax.fori_loop(0, 2 * NX, step, 0)
-        into[sp] = src[x, z]
+        into[sp] = src(x, z)[...]
 
     def wait_grads(into, which):
         landed(into.at[0 : NSP - 1], dpr.at[which])
@@ -341,11 +375,10 @@
             total = total + into[NX * h + xx].astype(F32)
         return total
 
-    def same(o, buf, which):
+    def along_y(o, slot_y, rows, buf, which):
         peer = rem4(y + o)
-        return remote(
-            buf.at[dp], buf.at[dp], as_.at[which], ar.at[which, y], dp=2 * peer + core
-        )
+        at = buf.at[2 * slot_y + core, rows]
+        return remote(at, at, as_.at[which], ar.at[which, slot_y], dp=2 * peer + core)
 
     def cross(yy, buf, which):
         slot = 2 * yy + core
@@ -354,19 +387,27 @@
         )
 
     def gather_start(buf, which):
-        for o in order:
-            same(o, buf, which).start()
+        along_y(1, y, slice(0, T), buf, which).start()
+        along_y(3, y, slice(0, T), buf, which).start()
         cross(y, buf, which).start()
 
-    def gather_finish(buf, which):
-        for o in order:
+    def gather_relay(buf, which):
+        for o in (1, 3):
             yy = rem4(y + o)
             landed(buf.at[0], ar.at[which, yy])
+            along_y(4 - o, yy, slice(0, 64) if o == 1 else slice(64, T), buf, which).start()
             cross(yy, buf, which).start()
+
+    def gather_last(buf, which):
+        yy = rem4(y + 2)
+        landed(buf.at[0], ar.at[which, yy])
+        cross(yy, buf, which).start()
+
+    def gather_finish(buf, which):
         landed(buf.at[0:4], ar.at[which, 4])
 
     def gi_src(peer):
-        return pb.at[pl.ds(pl.multiple_of(peer * T, T), T), 512:1024]
+        return li_all.at[peer]
 
     outs = (gwv, gwk)
 
@@ -376,7 +417,7 @@
         peer = rem4(me + o)
         wide = slice(half * 256, (half + 1) * 256)
         if stage == 0:
-            src = pb.at[pl.ds(pl.multiple_of(which * 512 + peer * T, T), T), wide]
+            src = pb.at[half, pl.ds(pl.multiple_of(which * 512 + peer * T, T), T)]
             dst = r1.at[which, half, me]
         elif stage == 1:
             src, dst = st1.at[which, half], r2.at[which, half, me]
@@ -401,7 +442,8 @@
 
     def reduce_start(buf, which):
         out = dot_tn(li_all[...].reshape(NDP * T, 512), buf[...].reshape(NDP * T, 512))
-        pb[which * 512 : (which + 1) * 512, 0:512] = out.astype(BF)
+        for half in range(2):
+            pb[half, which * 512 : (which + 1) * 512, :] = out[:, half * 256 : (half + 1) * 256].astype(BF)
         for half in range(2):
             stage_start(0, which, half)
 
@@ -410,7 +452,7 @@
             me = x if half == 0 else z
             stage_wait(0, which, half)
             at = pl.ds(pl.multiple_of(which * 512 + me * T, T), T)
-            total = pb[at, half * 256 : (half + 1) * 256].astype(F32)
+            total = pb[half, at].astype(F32)
             for o in order:
                 total = total + r1[which, half, rem4(me + o)].astype(F32)
             st1[which, half] = total.astype(BF)
@@ -428,16 +470,14 @@
             own_part(which, half).start()
 
     with jax.named_scope("s_dk"):
-        grads_out(ds, qs, dk_src, dk_in, 1)
-    with jax.named_scope("s_dv"):
-        grads_out(pb, gs, dv_src, dv_in, 0)
+        grads_out(ds, qs, lambda xx, zz: dk_src.at[xx, zz], dk_in, 1)
 
     def query_grads(i):
         off = i // 2
         zz = lax.rem(z + off, NZ)
         pair = lax.rem(i, 2)
         wide = pl.ds(pl.multiple_of(pair * 256, 256), 256)
-        grad = dot_nn(k_t[...], ds[:, block_cols(i)]).T * SCALE
+        grad = dot_nn(k_t[...], ds[i]).T * SCALE
         both = q_all[zz, :, wide].astype(F32)
         outs = []
         for h in range(2):
@@ -454,21 +494,32 @@
         zz = lax.rem(z + off, NZ)
         pair = lax.rem(i, 2)
 
-        @pl.when(i == 1)
-        def _():
-            pltpu.make_async_copy(dq_out.at[z], gq.at[:, cols(z, 512)], loc.at[6]).start()
-
-        @pl.when((pair == 1) & (off > 0))
-        def _():
-            dq_copy(zz).start()
+        if isinstance(i, int):
+            if i == 1:
+                pltpu.make_async_copy(dq_out.at[z], gq.at[:, cols(z, 512)], loc.at[6]).start()
+            else:
+                dq_copy(zz).start()
+        else:
+
+            @pl.when(pair == 1)
+            def _():
+                dq_copy(zz).start()
 
     def back(t, _):
         query_grads(t)
-        query_send(t)
+
+        @pl.when(t >= 4)
+        def _():
+            query_send(t)
+
         return 0
 
     with jax.named_scope("s_dq1"):
         lax.fori_loop(0, 4, back, 0)
+    with jax.named_scope("s_dv"):
+        grads_out(pb, gs, lambda xx, zz: g_all.at[xx, :, cols(zz, D)], dv_in, 0)
+    query_send(1)
+    query_send(3)
     with jax.named_scope("s_wdk"):
         wait_grads(dk_in, 1)
     pieces = []
@@ -482,6 +533,8 @@
 
     with jax.named_scope("s_dq2"):
         lax.fori_loop(4, 8, back, 0)
+    with jax.named_scope("s_rlk"):
+        gather_relay(ks_all, 1)
     with jax.named_scope("s_wdv"):
         wait_grads(dv_in, 0)
     vs_all[dp] = jnp.concatenate([head_sum(dv_in, h).astype(BF) for h in range(NZ)], axis=1)
@@ -490,13 +543,19 @@
 
     landed(li_all.at[0 : NDP - 1], misc.at[1])
     with jax.named_scope("s_gfk"):
+        gather_last(ks_all, 1)
         gather_finish(ks_all, 1)
     with jax.named_scope("s_rsk"):
         reduce_start(ks_all, 1)
     with jax.named_scope("s_gfv"):
+        gather_relay(vs_all, 0)
+        gather_last(vs_all, 0)
         gather_finish(vs_all, 0)
     with jax.named_scope("s_rsv"):
         reduce_start(vs_all, 0)
+
+    with jax.named_scope("s_rf1k"):
+        reduce_first(1)
 
     own[4].wait()
     own[5].wait()
@@ -509,7 +568,7 @@
         four = pl.ds(4 * group, 4)
         out = dot_nt(ks_all[four].reshape(512, 512), kw_s[...])
         out = out + dot_nt(vs_all[four].reshape(512, 512), vw_s[...])
-        pb[pl.ds(pl.multiple_of(group * 512, 512), 512), 512:1024] = out.astype(BF)
+        li_all[four] = out.astype(BF).reshape(4, T, 512)
         for j in range(4):
             peer = 4 * group + j
 
@@ -523,8 +582,7 @@
         lax.fori_loop(0, 2, grad_in, 0)
     pltpu.make_async_copy(gi_src(dp), gin.at[:, cols(dp, 512)], loc.at[16]).start()
 
-    with jax.named_scope("s_rf1"):
-        reduce_first(1)
+    with jax.named_scope("s_rf1v"):
         reduce_first(0)
     with jax.named_scope("s_rf2"):
         reduce_second(1)
@@ -624,12 +682,11 @@
             V((8, 2048), F32),
             V((8, 2048), F32),
             V((8, 2048), F32),
-            V((2048, 2048), F32),
-            V((2048, 2048), F32),
-            V((2048, 2048), BF),
-            V((2048, 2048), BF),
+            V((8, 2048, 256), F32),
+            V((8, 2048, 256), F32),
+            V((8, 2048, 256), BF),
+            V((8, 2048, 256), BF),
             V((NZ, T, 512), BF),
-            V((NX, NZ, T, D), BF),
             V((NX, NZ, T, D), BF),
             V((NSP, T, D), BF),
             V((NSP, T, D), BF),

time: 85.7 us -> 84 us (0.980)
  Pallas kernels: 84.8 us -> 83.2 us
    pallas_call x1, Pallas kernels: 81.8 us -> 80.1 us  [on_device(): pl.pallas_call(body, out_shape=(jax.ShapeDtypeStruct((T, 2048), BF), jax....]
where the time goes in v5:
time: 84 us; the launch traced here: 83.8 us
  Pallas kernels  83.2 us (99%)
    pallas_call x1, Pallas kernels, on_device(): pl.pallas_call(body, out_shape=(jax.ShapeDtypeStruct((T, 2048), BF), jax....  80.1 us
    pallas_call x1, Pallas kernels, on_device(): pl.pallas_call(finish, out_shape=(jax.ShapeDtypeStruct((T, 2048), BF), ja...  3.02 us

profile of v5, /device:TPU:1, one launch (start us, length us, event | category | flops | bytes accessed | tf_op | source)
XLA Modules:
  0.0 83.8 jit_solution(5811222327545060933)
XLA Ops:
  0.6 80.1 %step.1 = (bf16[128,2048]{1,0:T(8,128)(2,1)}, bf16[128,4096]{1,0:T(8,128)(2,1)}, bf16[512,512]{1,0:T(8,128)(2,1)}, bf16[512,512]{1,0:T(8,128)(2,1)}) custom-call(bf16[128,2048]{1,0:T(8,128)(2,1)} %bitcast.10, bf16[128,512]{1,0:T(8,128)(2,1)} %bitcast.12, bf16[128,512]{1,0:T(8,128)(2,1)} %bitcast.13, bf16[128,2048]{1,0:T(8,128)(2,1)} %bitcast.11, ...), custom_call_target="tpu_custom_call" | custom-call | tf_op jit(solution)/shard_map/step/pallas_call | solution.py:657
  80.8 3.0 %finish.1 = (bf16[128,2048]{1,0:T(8,128)(2,1)}, bf16[128,4096]{1,0:T(8,128)(2,1)}, f32[512,512]{1,0:T(8,128)}, f32[512,512]{1,0:T(8,128)}) custom-call(bf16[128,2048]{1,0:T(8,128)(2,1)} %get-tuple-element.12.gq_in, bf16[128,4096]{1,0:T(8,128)(2,1)} %get-tuple-element.13.gin_in, bf16[512,512]{1,0:T(8,128)(2,1)} %get-tuple-element.14.gwv_in, ...), custom_call_target="tpu_custom_call" | custom-call | tf_op jit(solution)/shard_map/finish/pallas_call | solution.py:723

commit v6 on v5

--- a/solution.py
+++ b/solution.py
@@ -427,7 +427,7 @@
         return remote(src, dst, ts.at[stage], trs.at[stage, which, half], sp=target)
 
     def stage_start(stage, which, half):
-        for o in order:
+        for o in (2, 1, 3):
             stage_copy(stage, which, half, o).start()
 
     def stage_wait(stage, which, half):

time: 84 us -> 83.6 us (level)
  no operation moved by 1% of the time
where the time goes in v6:
time: 83.6 us; the launch traced here: 83.5 us
  Pallas kernels  82.8 us (99%)
    pallas_call x1, Pallas kernels, on_device(): pl.pallas_call(body, out_shape=(jax.ShapeDtypeStruct((T, 2048), BF), jax....  79.8 us
    pallas_call x1, Pallas kernels, on_device(): pl.pallas_call(finish, out_shape=(jax.ShapeDtypeStruct((T, 2048), BF), ja...  3.02 us

profile of v6, /device:TPU:1, one launch (start us, length us, event | category | flops | bytes accessed | tf_op | source)
XLA Modules:
  0.0 83.5 jit_solution(15580047421441050512)
XLA Ops:
  0.6 79.8 %step.1 = (bf16[128,2048]{1,0:T(8,128)(2,1)}, bf16[128,4096]{1,0:T(8,128)(2,1)}, bf16[512,512]{1,0:T(8,128)(2,1)}, bf16[512,512]{1,0:T(8,128)(2,1)}) custom-call(bf16[128,2048]{1,0:T(8,128)(2,1)} %bitcast.10, bf16[128,512]{1,0:T(8,128)(2,1)} %bitcast.12, bf16[128,512]{1,0:T(8,128)(2,1)} %bitcast.13, bf16[128,2048]{1,0:T(8,128)(2,1)} %bitcast.11, ...), custom_call_target="tpu_custom_call" | custom-call | tf_op jit(solution)/shard_map/step/pallas_call | solution.py:657
  80.5 3.0 %finish.1 = (bf16[128,2048]{1,0:T(8,128)(2,1)}, bf16[128,4096]{1,0:T(8,128)(2,1)}, f32[512,512]{1,0:T(8,128)}, f32[512,512]{1,0:T(8,128)}) custom-call(bf16[128,2048]{1,0:T(8,128)(2,1)} %get-tuple-element.12.gq_in, bf16[128,4096]{1,0:T(8,128)(2,1)} %get-tuple-element.13.gin_in, bf16[512,512]{1,0:T(8,128)(2,1)} %get-tuple-element.14.gwv_in, ...), custom_call_target="tpu_custom_call" | custom-call | tf_op jit(solution)/shard_map/finish/pallas_call | solution.py:723

commit v7 on v6

--- a/solution.py
+++ b/solution.py
@@ -343,16 +343,14 @@
     k_t[...] = k_all[...].reshape(NSP * T, D).T
     def grads_out(left, right, src, into, which):
         def step(t, _):
-            xx = lax.rem(x + 1 + t // 2, NX)
-            half = lax.rem(t, 2)
-            at = pl.ds(pl.multiple_of(xx * 512 + half * 256, 256), 256)
+            xx = lax.rem(x + 1 + t, NX)
+            at = pl.ds(pl.multiple_of(xx * 512, 512), 512)
             out = dot_nn(left[0, at, :], right[0:256, :])
             for j in range(1, 8):
                 out = out + dot_nn(left[j, at, :], right[j * 256 : (j + 1) * 256, :])
-            for j in range(2):
-                src(xx, 2 * half + j)[...] = out[j * T : (j + 1) * T].astype(BF)
-            for j in range(2):
-                zz = 2 * half + j
+            for zz in range(NZ):
+                src(xx, zz)[...] = out[zz * T : (zz + 1) * T].astype(BF)
+            for zz in range(NZ):
                 peer = zz * NX + xx
 
                 @pl.when(peer != sp)
@@ -363,7 +361,7 @@
 
             return 0
 
-        lax.fori_loop(0, 2 * NX, step, 0)
+        lax.fori_loop(0, NX, step, 0)
         into[sp] = src(x, z)[...]
 
     def wait_grads(into, which):

time: 83.6 us -> 83.8 us (level)
  no operation moved by 1% of the time
where the time goes in v7:
time: 83.8 us; the launch traced here: 83.7 us
  Pallas kernels  83 us (99%)
    pallas_call x1, Pallas kernels, on_device(): pl.pallas_call(body, out_shape=(jax.ShapeDtypeStruct((T, 2048), BF), jax....  80 us
    pallas_call x1, Pallas kernels, on_device(): pl.pallas_call(finish, out_shape=(jax.ShapeDtypeStruct((T, 2048), BF), ja...  3.02 us

profile of v7, /device:TPU:1, one launch (start us, length us, event | category | flops | bytes accessed | tf_op | source)
XLA Modules:
  0.0 83.7 jit_solution(6145682231418232837)
XLA Ops:
  0.6 80.0 %step.1 = (bf16[128,2048]{1,0:T(8,128)(2,1)}, bf16[128,4096]{1,0:T(8,128)(2,1)}, bf16[512,512]{1,0:T(8,128)(2,1)}, bf16[512,512]{1,0:T(8,128)(2,1)}) custom-call(bf16[128,2048]{1,0:T(8,128)(2,1)} %bitcast.10, bf16[128,512]{1,0:T(8,128)(2,1)} %bitcast.12, bf16[128,512]{1,0:T(8,128)(2,1)} %bitcast.13, bf16[128,2048]{1,0:T(8,128)(2,1)} %bitcast.11, ...), custom_call_target="tpu_custom_call" | custom-call | tf_op jit(solution)/shard_map/step/pallas_call | solution.py:655
  80.7 3.0 %finish.1 = (bf16[128,2048]{1,0:T(8,128)(2,1)}, bf16[128,4096]{1,0:T(8,128)(2,1)}, f32[512,512]{1,0:T(8,128)}, f32[512,512]{1,0:T(8,128)}) custom-call(bf16[128,2048]{1,0:T(8,128)(2,1)} %get-tuple-element.12.gq_in, bf16[128,4096]{1,0:T(8,128)(2,1)} %get-tuple-element.13.gin_in, bf16[512,512]{1,0:T(8,128)(2,1)} %get-tuple-element.14.gwv_in, ...), custom_call_target="tpu_custom_call" | custom-call | tf_op jit(solution)/shard_map/finish/pallas_call | solution.py:721
